TPU v7x, 32 devices: a whole 2x2x4 slice. The times are simulated.
32 devices in a mesh: grp: 2 (over y), sp: 4 (over z), tp: 4 (over x, core).
Axes of the slice: x: 2, y: 2, z: 4, core: 2. Of those that a mesh axis runs over, the one named last changes fastest.
Arguments:
- resid_in: bfloat16 [2048, 2048], P(('grp', 'sp', 'tp')), parts along dimension 0, may hold values from -3 to 3
- queries: bfloat16 [2048, 1024], P(('grp', 'sp'), 'tp'), parts along dimension 0, may hold values from -39 to 39
- keys: bfloat16 [2048, 1024], P(('grp', 'sp'), 'tp'), parts along dimension 0, may hold values from -6 to 6
- values: bfloat16 [2048, 1024], P(('grp', 'sp'), 'tp'), parts along dimension 0, may hold values from -12 to 12
- cum_gate: float32 [2048, 16], P('grp', 'tp'), parts along dimension 0, may hold values from -105 to 0, as said below
- w_out: bfloat16 [1024, 2048], replicated, may hold values from -0.1875 to 0.1875
- norm_gain: float32 [2048], replicated, may hold values from 0.1 to 1.9
- w_gate: bfloat16 [2048, 5632], P('sp', 'tp'), may hold values from -0.125 to 0.125
- w_up: bfloat16 [2048, 5632], P('sp', 'tp'), may hold values from -0.125 to 0.125
- w_down: bfloat16 [5632, 2048], P('tp', 'sp'), may hold values from -0.078125 to 0.078125
Outputs:
- resid_out: bfloat16 [2048, 2048], P(('grp', 'sp', 'tp')), parts along dimension 0
There are 2 independent parts, one for each index of `grp`. A program takes and returns all parts, laid end to end along the dimension named above; an argument that names none is the same for every part. Nothing has to cross between parts.
Inputs may be any that keep to these rules, and one draw needn't show every extreme that they name: `cum_gate`: in every head the values never rise from one position to the next, and the first is at most 0.
All inputs are finite; a program needn't handle non-finite values.
Results may differ from a plain program's by a relative error of at most 0.018.
Values may be sent and summed in bfloat16 or wider, within the bound.
A program may use at most 128 MiB of HBM per device.

v0:
```python
import functools
import math

import jax
import jax.numpy as jnp
from jax import lax
from jax.experimental import pallas as pl
from jax.experimental.pallas import tpu as pltpu
from jax.sharding import PartitionSpec as P

HEAD_DIM = 64


def on_device(resid_in, queries, keys, values, cum_gate, w_out, norm_gain, w_gate, w_up, w_down):
    tok_rows = queries.shape[0]
    local_heads = queries.shape[1] // HEAD_DIM
    scale = HEAD_DIM ** (-0.5)
    offset = lax.axis_index("sp") * tok_rows
    query_heads = queries.reshape(tok_rows, local_heads, HEAD_DIM)
    own_gate = lax.dynamic_slice_in_dim(cum_gate, offset, tok_rows, 0).T
    query_pos = offset + jnp.arange(tok_rows, dtype=jnp.int32)
    last_pos = offset + tok_rows - 1
    initial = (
        jnp.full((local_heads, tok_rows), -1e30, jnp.float32),
        jnp.zeros((local_heads, tok_rows), jnp.float32),
        jnp.zeros((tok_rows, local_heads, HEAD_DIM), jnp.float32),
    )
    pair = lax.all_gather(jnp.stack([keys, values]), "sp", axis=1, tiled=True)
    key_piece, value_piece = pair[0], pair[1]
    length = key_piece.shape[0]
    span = math.gcd(length, 512)

    def block(index, state):
        begin = index * span

        def work(inner):
            maxima, totals, summed = inner
            key_block = lax.dynamic_slice_in_dim(key_piece, index * span, span, 0).reshape(
                span, local_heads, HEAD_DIM
            )
            value_block_rows = lax.dynamic_slice_in_dim(value_piece, index * span, span, 0).reshape(
                span, local_heads, HEAD_DIM
            )
            key_gate = lax.dynamic_slice_in_dim(cum_gate, begin, span, 0).T
            scores = (
                jnp.einsum(
                    "qhd,khd->hqk", query_heads, key_block, preferred_element_type=jnp.float32
                )
                * scale
            )
            scores = scores + own_gate[:, :, None] - key_gate[:, None, :]
            key_pos = begin + jnp.arange(span, dtype=jnp.int32)
            mask = (key_pos[None, :] <= query_pos[:, None])[None]
            scores = jnp.where(mask, scores, -1e30)
            new_max = jnp.maximum(maxima, jnp.max(scores, axis=-1))
            weights = jnp.where(mask, jnp.exp(scores - new_max[:, :, None]), 0.0)
            rescale = jnp.exp(maxima - new_max)
            totals = totals * rescale + jnp.sum(weights, axis=-1)
            product = jnp.einsum(
                "hqk,khd->qhd",
                weights.astype(jnp.bfloat16),
                value_block_rows,
                preferred_element_type=jnp.float32,
            )
            summed = summed * rescale.T[:, :, None] + product
            return (new_max, totals, summed)

        return lax.cond(begin <= last_pos, work, lambda inner: inner, state)

    maxima, totals, summed = lax.fori_loop(0, length // span, block, initial)
    attended = (
        (summed / totals.T[:, :, None])
        .reshape(tok_rows, local_heads * HEAD_DIM)
        .astype(jnp.bfloat16)
    )
    head_rows = lax.all_to_all(attended, "tp", split_axis=0, concat_axis=1, tiled=True)
    mixed = jnp.dot(head_rows, w_out, preferred_element_type=jnp.float32)
    resid = resid_in.astype(jnp.float32) + mixed
    normed = resid * lax.rsqrt(jnp.mean(resid * resid, axis=-1, keepdims=True) + 1e-06)
    normed = (normed * norm_gain).astype(jnp.bfloat16)
    all_rows = lax.all_gather(normed, ("sp", "tp"), axis=0, tiled=True)
    full_gate, full_up, full_down = (
        lax.all_to_all(w_gate, "sp", split_axis=1, concat_axis=0, tiled=True),
        lax.all_to_all(w_up, "sp", split_axis=1, concat_axis=0, tiled=True),
        lax.all_to_all(w_down, "sp", split_axis=0, concat_axis=1, tiled=True),
    )
    gate = jnp.dot(all_rows, full_gate, preferred_element_type=jnp.float32)
    up = jnp.dot(all_rows, full_up, preferred_element_type=jnp.float32)
    hidden = (jax.nn.silu(gate) * up).astype(jnp.bfloat16)
    terms = jnp.dot(hidden, full_down, preferred_element_type=jnp.float32)
    back = lax.psum_scatter(
        terms.astype(jnp.bfloat16), ("sp", "tp"), scatter_dimension=0, tiled=True
    ).astype(jnp.float32)
    return (resid + back).astype(jnp.bfloat16)


MESH = pl.DeviceIdType.MESH
F32 = jnp.float32
BF16 = jnp.bfloat16


def layer_kernel(
    dims, resid_ref, q_ref, k_ref, v_ref, gate_t_ref, gain_ref, w_out_ref, w_gate_ref,
    w_up_ref, w_down_ref, out_ref, kbuf, vbuf, top, tot, acc, att, heads, w_out, resid, nall, wg,
    wu, wd, hidden, part, crecv, csend, keep, xrecv, zsend, zrecv, loc_sem, kv_send, kv_recv, wz_send,
    wz_recv, wy_send, wy_recv, h_send, h_recv, az_send, az_recv, ax_send, ax_recv, ac_send,
    ac_recv, rc_send, rc_recv, rx_send, rx_recv, rz_send, rz_recv, go,
):
    ns, nt, chunk = dims
    g, s, t = lax.axis_index("grp"), lax.axis_index("sp"), lax.axis_index("tp")
    rows, width = resid_ref.shape
    tok, att_w = q_ref.shape
    depth, units = w_gate_ref.shape
    nheads = att_w // HEAD_DIM
    half_depth = depth // 2
    dup = ns * chunk - units
    x, c = t // 2, t % 2
    tx = (t + 2) % 4
    tc = t + 1 - 2 * c
    scale = HEAD_DIM ** (-0.5)

    def start_of(i):
        return pl.multiple_of(jnp.minimum(i * chunk, units - chunk), 128)

    def remote(src, dst, send, recv, **where):
        return pltpu.make_async_remote_copy(
            src_ref=src, dst_ref=dst, send_sem=send, recv_sem=recv, device_id=where,
            device_id_type=MESH,
        )

    def xor(a, b):
        hi, lo, bh, bl = a // 2, a % 2, b // 2, b % 2
        return 2 * (hi + bh - 2 * hi * bh) + lo + bl - 2 * lo * bl

    def landing(mat, src, half, skip):
        if mat < 2:
            return (wg, wu)[mat].at[
                pl.ds(pl.multiple_of(src * depth + half * half_depth, half_depth), half_depth),
                pl.ds(skip, chunk - skip),
            ]
        size = (chunk - skip) // 2
        return wd.at[
            pl.ds(pl.multiple_of(skip + half * size, math.gcd(128, size)), size),
            pl.ds(pl.multiple_of(src * depth, depth), depth),
        ]

    def weight_out(mat, dst, skip):
        if mat < 2:
            src = (w_gate_ref, w_up_ref)[mat].at[
                pl.ds(pl.multiple_of(g * half_depth, half_depth), half_depth),
                pl.ds(pl.multiple_of(start_of(dst) + skip, 128), chunk - skip),
            ]
        else:
            size = (chunk - skip) // 2
            src = w_down_ref.at[
                pl.ds(pl.multiple_of(start_of(dst) + skip + g * size, math.gcd(128, size)), size)
            ]
        return remote(
            src, landing(mat, s, g, skip), wz_send.at[mat, dst], wz_recv.at[mat, s], sp=dst
        )

    def weight_in(mat, src, skip):
        block = landing(mat, src, g, skip)
        return remote(block, block, wz_send.at[mat, src], wz_recv.at[mat, src], sp=src)

    def weight_pass(mat, src, half, skip):
        block = landing(mat, src, half, skip)
        return remote(block, block, wy_send.at[mat, src], wy_recv.at[mat, src], grp=1 - g)

    def sized(dst, body):
        pl.when(dst < ns - 1)(lambda: body(0))
        pl.when(dst == ns - 1)(lambda: body(dup))

    def each(low, high, body):
        lax.fori_loop(low, high, lambda i, z: (body(i), z)[1], 0)

    def others(body):
        each(0, s, body)
        each(s + 1, ns, body)

    barrier = pltpu.get_barrier_semaphore()
    others(lambda i: pl.semaphore_signal(barrier, inc=1, device_id={"sp": i}, device_id_type=MESH))
    pl.semaphore_signal(barrier, inc=1, device_id={"grp": 1 - g}, device_id_type=MESH)
    for j in range(1, nt):
        pl.semaphore_signal(barrier, inc=1, device_id={"tp": (t + j) % nt}, device_id_type=MESH)
    pl.semaphore_wait(barrier, ns + nt - 1)

    def kv_out(i, kk, vv):
        return (
            remote(kk, kbuf.at[i], kv_send.at[0, i], kv_recv.at[0, i], sp=s + 1),
            remote(vv, vbuf.at[i], kv_send.at[1, i], kv_recv.at[1, i], sp=s + 1),
        )

    def kv_in(i):
        return (
            remote(kbuf.at[i], kbuf.at[i], kv_send.at[0, i], kv_recv.at[0, i], sp=s - 1),
            remote(vbuf.at[i], vbuf.at[i], kv_send.at[1, i], kv_recv.at[1, i], sp=s - 1),
        )

    @pl.when(s + 1 < ns)
    def _():
        for copy in kv_out(0, k_ref, v_ref):
            copy.start()

    def locals_():
        own = pl.ds(pl.multiple_of(s * depth, depth), depth)
        return (
            pltpu.make_async_copy(w_out_ref, w_out, loc_sem.at[0]),
            pltpu.make_async_copy(w_gate_ref.at[:, pl.ds(start_of(s), chunk)], wg.at[own], loc_sem.at[1]),
            pltpu.make_async_copy(w_up_ref.at[:, pl.ds(start_of(s), chunk)], wu.at[own], loc_sem.at[2]),
            pltpu.make_async_copy(w_down_ref.at[pl.ds(start_of(s), chunk)], wd.at[:, own], loc_sem.at[3]),
        )

    for copy in locals_():
        copy.start()
    def send_weight(mat, dst):
        sized(dst, lambda skip: weight_out(mat, dst, skip).start())

    for mat in range(2):
        each(0, s, lambda i, mat=mat: send_weight(mat, s - 1 - i))

    if dup:

        @pl.when(s == ns - 1)
        def _():
            for mat in range(2):
                def clear(i, mat=mat):
                    band = pl.ds(pl.multiple_of((i + (i >= s)) * depth, depth), depth)
                    (wg, wu)[mat][band, :dup] = jnp.zeros((depth, dup), BF16)

                each(0, ns - 1, clear)
            wd[:dup, : (ns - 1) * depth] = jnp.zeros((dup, (ns - 1) * depth), BF16)

    gate_own = gate_t_ref[:, pl.ds(pl.multiple_of(s * tok, tok), tok)].T

    def attend(src, kk, vv, first):
        for h in range(nheads):
            lanes = slice(h * HEAD_DIM, (h + 1) * HEAD_DIM)
            scores = lax.dot_general(
                q_ref[:, lanes], kk[:, lanes], (((1,), (1,)), ((), ())), preferred_element_type=F32
            )
            key_gate = gate_t_ref[h : h + 1, pl.ds(pl.multiple_of(src * tok, tok), tok)]
            scores = scores * scale + gate_own[:, h : h + 1] - key_gate
            if first:
                row = lax.broadcasted_iota(jnp.int32, (tok, tok), 0)
                col = lax.broadcasted_iota(jnp.int32, (tok, tok), 1)
                scores = jnp.where(col <= row, scores, -1e30)
                new = jnp.max(scores, axis=-1, keepdims=True)
                w = jnp.where(col <= row, jnp.exp(scores - new), 0.0)
                tot[h] = jnp.sum(w, axis=-1, keepdims=True)
                acc[h] = jnp.dot(w.astype(BF16), vv[:, lanes], preferred_element_type=F32)
            else:
                old = top[h]
                new = jnp.maximum(old, jnp.max(scores, axis=-1, keepdims=True))
                w = jnp.exp(scores - new)
                shrink = jnp.exp(old - new)
                tot[h] = tot[h] * shrink + jnp.sum(w, axis=-1, keepdims=True)
                acc[h] = acc[h] * shrink + jnp.dot(
                    w.astype(BF16), vv[:, lanes], preferred_element_type=F32
                )
            top[h] = new

    attend(s, k_ref, v_ref, True)

    def earlier(i):
        for copy in kv_in(i - 1):
            copy.wait_recv()

        @pl.when(s + 1 < ns)
        def _():
            for copy in kv_out(i, kbuf.at[i - 1], vbuf.at[i - 1]):
                copy.start()

        @pl.when((i == s) & (s == ns - 2))
        def _():
            each(
                0, s,
                lambda j: pl.semaphore_signal(
                    go, inc=1, device_id={"sp": j}, device_id_type=MESH
                ),
            )

        attend(s - i, kbuf.at[i - 1], vbuf.at[i - 1], False)

    each(1, s + 1, earlier)

    for h in range(nheads):
        att[:, h * HEAD_DIM : (h + 1) * HEAD_DIM] = (acc[h] / tot[h]).astype(BF16)

    def head_copy(j):
        dst = (t + j) % nt
        return remote(
            att.at[pl.ds(pl.multiple_of(dst * rows, rows), rows)], heads.at[j - 1],
            h_send.at[j - 1], h_recv.at[j - 1], tp=dst,
        )

    for j in range(1, nt):
        head_copy(j).start()

    def pass_on(mat, src):
        def body(skip):
            weight_in(mat, src, skip).wait_recv()
            weight_pass(mat, src, g, skip).start()

        sized(s, body)

    copies = locals_()
    copies[0].wait()
    resid[...] = resid_ref[...].astype(F32) + jnp.dot(
        att[pl.ds(pl.multiple_of(t * rows, rows), rows), :],
        w_out[pl.ds(pl.multiple_of(t * att_w, att_w), att_w), :], preferred_element_type=F32,
    )

    def mix(j):
        head_copy(j).wait_recv()
        src = (t + nt - j) % nt
        resid[...] += jnp.dot(
            heads[j - 1], w_out[pl.ds(pl.multiple_of(src * att_w, att_w), att_w), :],
            preferred_element_type=F32,
        )

    each(1, nt, mix)
    full = resid[...]
    normed = full * lax.rsqrt(jnp.mean(full * full, axis=-1, keepdims=True) + 1e-06)
    nall[s, t] = (normed * gain_ref[...]).astype(BF16)

    def row_z(src, to):
        block = nall.at[src, t]
        return remote(block, block, az_send.at[0, src], az_recv.at[src], sp=to)

    def row_far(to):
        block = nall.at[s, t]
        return remote(block, block, az_send.at[1, s], az_recv.at[s], sp=to)

    def row_x(src, who):
        block = nall.at[src, who]
        return remote(block, block, ax_send.at[src], ax_recv.at[src], tp=tx)

    def row_c(kind, src, who):
        block = nall.at[src, who]
        return remote(block, block, ac_send.at[kind, src], ac_recv.at[kind, src], tp=tc)

    def spread(src):
        row_x(src, t).start()
        row_c(0, src, t).start()

    def relay(src):
        row_x(src, tx).wait_recv()
        row_c(1, src, tx).start()

    near, far, cross = xor(s, 1), xor(s, 2), xor(s, 3)
    pl.when(s < ns - 2)(lambda: pl.semaphore_wait(go, 1))
    row_far(far).start()
    row_z(s, near).start()
    for mat in range(2):
        each(s + 1, ns, lambda i, mat=mat: send_weight(mat, i))
    each(0, s, lambda i: send_weight(2, s - 1 - i))
    each(s + 1, ns, lambda i: send_weight(2, i))
    spread(s)

    def take_far():
        row_z(far, far).wait_recv()
        row_z(far, near).start()
        spread(far)

    def take(src):
        row_z(src, near).wait_recv()
        spread(src)

    for mat in range(2):
        each(s + 1, ns, lambda i, mat=mat: pass_on(mat, i))
    relay(s)
    pl.when(s >= 2)(take_far)
    for mat in range(2):
        each(0, s, lambda i, mat=mat: pass_on(mat, s - 1 - i))
    pl.when(s < 2)(take_far)
    take(near)
    relay(far)
    take(cross)
    each(s + 1, ns, lambda i: pass_on(2, i))
    each(0, s, lambda i: pass_on(2, s - 1 - i))
    relay(near)
    relay(cross)

    for copy in copies[1:]:
        copy.wait()

    def twin_in(mat):
        others(lambda i: sized(s, lambda skip: weight_pass(mat, i, 1 - g, skip).wait_recv()))

    twin_in(0)
    twin_in(1)
    fresh = lax.broadcasted_iota(jnp.int32, (tok, chunk), 1) + start_of(s) >= s * chunk
    half = width // 2
    piece = math.gcd(half, 512)

    def hide(src):
        row_c(0, src, tc).wait_recv()
        row_c(1, src, (tc + 2) % 4).wait_recv()
        a = nall[src].reshape(tok, width)
        gate = jnp.dot(a, wg[...], preferred_element_type=F32)
        up = jnp.dot(a, wu[...], preferred_element_type=F32)
        hidden[src] = jnp.where(fresh, gate / (1.0 + jnp.exp(-gate)) * up, 0.0).astype(BF16)

    each(0, ns, lambda k: hide(xor(s, k)))
    twin_in(2)

    def sum_c(d):
        return remote(part.at[d, :, 1 - c], crecv.at[d], rc_send.at[d], rc_recv.at[d], tp=tc)

    def sum_x(d):
        return remote(csend.at[d], xrecv.at[d], rx_send.at[d], rx_recv.at[d], tp=tx)

    def sum_z(d):
        return remote(zsend.at[d], zrecv.at[d], rz_send.at[d], rz_recv.at[d], sp=xor(s, 1 + d // 2 % 2))

    def stage_x(d):
        sum_c(d).wait_recv()
        csend[d] = (part[d, 1 - x, c].astype(F32) + crecv[d, 1 - x].astype(F32)).astype(BF16)
        sum_x(d).start()
        keep[d] = part[d, x, c].astype(F32) + crecv[d, x].astype(F32)

    def stage_z(d):
        sum_x(d).wait_recv()
        keep[d] = keep[d] + xrecv[d].astype(F32)

        @pl.when((d == 2) | (d == 3))
        def _():
            sum_z(d - 2).wait_recv()
            keep[d] = keep[d] + zrecv[d - 2].astype(F32)

        zsend[d] = keep[d].astype(BF16)
        sum_z(d).start()

    def feed(d):
        src = hidden[xor(s, 3 - d // 2)]

        def down(p):
            cols = pl.ds(pl.multiple_of(p * piece, piece), piece)
            from_ = pl.ds(pl.multiple_of(d % 2 * half + p * piece, piece), piece)
            y = jnp.dot(src, wd[:, from_], preferred_element_type=F32).astype(BF16)
            part[d, :, :, :, cols] = y.reshape(2, 2, rows, piece)

        each(0, half // piece, down)
        sum_c(d).start()
        pl.when(d >= 1)(lambda: stage_x(d - 1))
        pl.when(d >= 3)(lambda: stage_z(d - 3))

    each(0, 2 * ns, feed)
    stage_x(2 * ns - 1)
    stage_z(2 * ns - 3)
    for d in (6, 7):
        cols = slice((d - 6) * half, (d - 5) * half)
        sum_x(d).wait_recv()
        sum_z(d - 4).wait_recv()
        sum_z(d - 2).wait_recv()
        resid[:, cols] += (
            keep[d] + xrecv[d].astype(F32) + zrecv[d - 4].astype(F32) + zrecv[d - 2].astype(F32)
        )
    out_ref[...] = resid[...].astype(BF16)

    @pl.when(s + 1 < ns)
    def _():
        def sent(i):
            for copy in kv_out(i, kbuf.at[0], vbuf.at[0]):
                copy.wait_send()

        each(0, s + 1, sent)

    row_far(far).wait_send()
    row_z(s, near).wait_send()
    row_z(far, near).wait_send()
    for mat in range(3):
        others(lambda i, mat=mat: sized(i, lambda skip: weight_out(mat, i, skip).wait_send()))
        others(lambda i, mat=mat: sized(s, lambda skip: weight_pass(mat, i, g, skip).wait_send()))
    for j in range(1, nt):
        head_copy(j).wait_send()

    def spread_done(i):
        row_x(i, t).wait_send()
        row_c(0, i, t).wait_send()
        row_c(1, i, tx).wait_send()

    each(0, ns, spread_done)

    def sums_done(d):
        sum_c(d).wait_send()
        sum_x(d).wait_send()

    each(0, 2 * ns, sums_done)
    each(0, 2 * ns - 2, lambda d: sum_z(d).wait_send())


def fused(ns, nt, chunk, resid_in, queries, keys, values, cum_gate, w_out, norm_gain, w_gate, w_up, w_down):
    rows, width = resid_in.shape
    tok, att_w = queries.shape
    depth, units = w_gate.shape
    nheads = att_w // HEAD_DIM
    vm = pl.BlockSpec(memory_space=pltpu.VMEM)
    hbm = pl.BlockSpec(memory_space=pltpu.HBM)
    dma = pltpu.SemaphoreType.DMA
    return pl.pallas_call(
        functools.partial(layer_kernel, (ns, nt, chunk)),
        out_shape=jax.ShapeDtypeStruct((rows, width), BF16),
        in_specs=[vm] * 6 + [hbm] * 4,
        out_specs=vm,
        scratch_shapes=[
            pltpu.VMEM((ns - 1, tok, att_w), BF16),
            pltpu.VMEM((ns - 1, tok, att_w), BF16),
            pltpu.VMEM((nheads, tok, 1), F32),
            pltpu.VMEM((nheads, tok, 1), F32),
            pltpu.VMEM((nheads, tok, HEAD_DIM), F32),
            pltpu.VMEM((tok, att_w), BF16),
            pltpu.VMEM((nt - 1, rows, att_w), BF16),
            pltpu.VMEM(w_out.shape, BF16),
            pltpu.VMEM((rows, width), F32),
            pltpu.VMEM((ns, nt, rows, width), BF16),
            pltpu.VMEM((width, chunk), BF16),
            pltpu.VMEM((width, chunk), BF16),
            pltpu.VMEM((chunk, width), BF16),
            pltpu.VMEM((ns, tok, chunk), BF16),
            pltpu.VMEM((2 * ns, 2, 2, rows, width // 2), BF16),
            pltpu.VMEM((2 * ns, 2, rows, width // 2), BF16),
            pltpu.VMEM((2 * ns, rows, width // 2), BF16),
            pltpu.VMEM((2 * ns, rows, width // 2), F32),
            pltpu.VMEM((2 * ns, rows, width // 2), BF16),
            pltpu.VMEM((2 * ns, rows, width // 2), BF16),
            pltpu.VMEM((2 * ns, rows, width // 2), BF16),
            dma((4,)),
            dma((2, ns)), dma((2, ns)),
            dma((3, ns)), dma((3, ns)),
            dma((3, ns)), dma((3, ns)),
            dma((nt - 1,)), dma((nt - 1,)),
            dma((2, ns)), dma((ns,)),
            dma((ns,)), dma((ns,)),
            dma((2, ns)), dma((2, ns)),
            dma((2 * ns,)), dma((2 * ns,)),
            dma((2 * ns,)), dma((2 * ns,)),
            dma((2 * ns,)), dma((2 * ns,)),
            pltpu.SemaphoreType.REGULAR,
        ],
        compiler_params=pltpu.CompilerParams(
            collective_id=0, has_side_effects=True, vmem_limit_bytes=60 * 2**20
        ),
        name="layer",
    )(
        resid_in, queries, keys, values, cum_gate.T, norm_gain[None, :], w_out, w_gate,
        w_up, w_down,
    )


def pick(mesh):
    ng, ns, nt = (mesh.shape[a] for a in ("grp", "sp", "tp"))

    def step(*args):
        resid_in, queries, cum_gate, w_gate = args[0], args[1], args[4], args[7]
        rows, width = resid_in.shape
        depth, units = w_gate.shape
        chunk = -(-units // (128 * ns)) * 128
        need = 2 * ns * nt * rows * width * 4 + 6 * width * chunk + 2 * args[5].size
        fits = (
            ng == 2 and nt == 4 and ns == 4 and units % 128 == 0 and (ns - 1) * chunk < units
            and depth % 256 == 0 and width % 256 == 0 and (chunk - ns * chunk + units) % 32 == 0 and width == ns * depth and rows % 16 == 0
            and queries.shape[0] == rows * nt and queries.shape[0] % 128 == 0
            and cum_gate.shape[0] == ns * nt * rows and queries.shape[1] % 128 == 0
            and need < 40 * 2**20
        )
        if fits:
            return fused(ns, nt, chunk, *args)
        return on_device(*args)

    return step


def solution(mesh):
    return jax.shard_map(
        pick(mesh),
        mesh=mesh,
        in_specs=(
            P(("grp", "sp", "tp"), None),
            P(("grp", "sp"), "tp"),
            P(("grp", "sp"), "tp"),
            P(("grp", "sp"), "tp"),
            P("grp", "tp"),
            P(),
            P(),
            P("sp", "tp"),
            P("sp", "tp"),
            P("tp", "sp"),
        ),
        out_specs=P(("grp", "sp", "tp"), None),
        check_vma=False,
    )
```

profile of v0, /device:TPU:0, one launch (start us, length us, event | category | flops | bytes accessed | tf_op | source)
XLA Modules:
  0.0 118.9 jit_solution(13275806223400138188)
XLA Ops:
  0.0 117.3 %layer.1 = bf16[64,2048]{1,0:T(8,128)(2,1)} custom-call(bf16[64,2048]{1,0:T(8,128)(2,1)} %resid_ref.1, bf16[256,256]{1,0:T(8,128)(2,1)} %q_ref.1, bf16[256,256]{1,0:T(8,128)(2,1)} %k_ref.1, bf16[256,256]{1,0:T(8,128)(2,1)} %v_ref.1, f32[4,1024]{1,0:T(4,128)} %bitcast.2, f32[1,2048]{1,0:T(1,128)} %bitcast.3, bf16[1024,2048]{1,0:T(8,128)(2,1)} %w_out_ref.1, ...), custom_call_target="tpu_custom_call" | custom-call | tf_op jit(solution)/shard_map/layer/pallas_call | solution.py:502
  117.3 1.7 %copy.12 = bf16[64,2048]{1,0:T(8,128)(2,1)} copy(bf16[64,2048]{1,0:T(8,128)(2,1)} %layer.1) | data formatting | bytes 524288
where the time goes:
time: 119 us
  Pallas kernels  117 us (98%)
  local copies, waits for them, and re-layouts  1.67 us (1%)
    pallas_call x1, Pallas kernels, fused(): pl.pallas_call(functools.partial(layer_kernel, (ns, nt, chunk)), out_shap...  117 us

commit v1 on v0

v1 whole, which is shorter than its diff:
```python
import functools
import math

import jax
import jax.numpy as jnp
from jax import lax
from jax.experimental import pallas as pl
from jax.experimental.pallas import tpu as pltpu
from jax.sharding import PartitionSpec as P

HEAD_DIM = 64


def on_device(resid_in, queries, keys, values, cum_gate, w_out, norm_gain, w_gate, w_up, w_down):
    tok_rows = queries.shape[0]
    local_heads = queries.shape[1] // HEAD_DIM
    scale = HEAD_DIM ** (-0.5)
    offset = lax.axis_index("sp") * tok_rows
    query_heads = queries.reshape(tok_rows, local_heads, HEAD_DIM)
    own_gate = lax.dynamic_slice_in_dim(cum_gate, offset, tok_rows, 0).T
    query_pos = offset + jnp.arange(tok_rows, dtype=jnp.int32)
    last_pos = offset + tok_rows - 1
    initial = (
        jnp.full((local_heads, tok_rows), -1e30, jnp.float32),
        jnp.zeros((local_heads, tok_rows), jnp.float32),
        jnp.zeros((tok_rows, local_heads, HEAD_DIM), jnp.float32),
    )
    pair = lax.all_gather(jnp.stack([keys, values]), "sp", axis=1, tiled=True)
    key_piece, value_piece = pair[0], pair[1]
    length = key_piece.shape[0]
    span = math.gcd(length, 512)

    def block(index, state):
        begin = index * span

        def work(inner):
            maxima, totals, summed = inner
            key_block = lax.dynamic_slice_in_dim(key_piece, index * span, span, 0).reshape(
                span, local_heads, HEAD_DIM
            )
            value_block_rows = lax.dynamic_slice_in_dim(value_piece, index * span, span, 0).reshape(
                span, local_heads, HEAD_DIM
            )
            key_gate = lax.dynamic_slice_in_dim(cum_gate, begin, span, 0).T
            scores = (
                jnp.einsum(
                    "qhd,khd->hqk", query_heads, key_block, preferred_element_type=jnp.float32
                )
                * scale
            )
            scores = scores + own_gate[:, :, None] - key_gate[:, None, :]
            key_pos = begin + jnp.arange(span, dtype=jnp.int32)
            mask = (key_pos[None, :] <= query_pos[:, None])[None]
            scores = jnp.where(mask, scores, -1e30)
            new_max = jnp.maximum(maxima, jnp.max(scores, axis=-1))
            weights = jnp.where(mask, jnp.exp(scores - new_max[:, :, None]), 0.0)
            rescale = jnp.exp(maxima - new_max)
            totals = totals * rescale + jnp.sum(weights, axis=-1)
            product = jnp.einsum(
                "hqk,khd->qhd",
                weights.astype(jnp.bfloat16),
                value_block_rows,
                preferred_element_type=jnp.float32,
            )
            summed = summed * rescale.T[:, :, None] + product
            return (new_max, totals, summed)

        return lax.cond(begin <= last_pos, work, lambda inner: inner, state)

    maxima, totals, summed = lax.fori_loop(0, length // span, block, initial)
    attended = (
        (summed / totals.T[:, :, None])
        .reshape(tok_rows, local_heads * HEAD_DIM)
        .astype(jnp.bfloat16)
    )
    head_rows = lax.all_to_all(attended, "tp", split_axis=0, concat_axis=1, tiled=True)
    mixed = jnp.dot(head_rows, w_out, preferred_element_type=jnp.float32)
    resid = resid_in.astype(jnp.float32) + mixed
    normed = resid * lax.rsqrt(jnp.mean(resid * resid, axis=-1, keepdims=True) + 1e-06)
    normed = (normed * norm_gain).astype(jnp.bfloat16)
    all_rows = lax.all_gather(normed, ("sp", "tp"), axis=0, tiled=True)
    full_gate, full_up, full_down = (
        lax.all_to_all(w_gate, "sp", split_axis=1, concat_axis=0, tiled=True),
        lax.all_to_all(w_up, "sp", split_axis=1, concat_axis=0, tiled=True),
        lax.all_to_all(w_down, "sp", split_axis=0, concat_axis=1, tiled=True),
    )
    gate = jnp.dot(all_rows, full_gate, preferred_element_type=jnp.float32)
    up = jnp.dot(all_rows, full_up, preferred_element_type=jnp.float32)
    hidden = (jax.nn.silu(gate) * up).astype(jnp.bfloat16)
    terms = jnp.dot(hidden, full_down, preferred_element_type=jnp.float32)
    back = lax.psum_scatter(
        terms.astype(jnp.bfloat16), ("sp", "tp"), scatter_dimension=0, tiled=True
    ).astype(jnp.float32)
    return (resid + back).astype(jnp.bfloat16)


MESH = pl.DeviceIdType.MESH
F32 = jnp.float32
BF16 = jnp.bfloat16
UNIT = 128
PIECES = 4


def layer_kernel(
    dims, resid_ref, q_ref, k_ref, v_ref, gate_t_ref, gain_ref, w_out_ref, w_gate_ref,
    w_up_ref, w_down_ref, out_ref, kbuf, vbuf, top, tot, acc, att, heads, w_out, resid, nall, wgu,
    wd, hidden, part, crecv, csend, keep, xrecv, zsend, zrecv, loc_sem, kv_send, kv_recv, wz_send,
    wz_recv, wy_send, wy_recv, dz_send, dz_recv, dy_send, dy_recv, h_send, h_recv, az_send, az_recv,
    ax_send, ax_recv, ac_send, ac_recv, rc_send, rc_recv, rx_send, rx_recv, rz_send, rz_recv,
):
    ns, nt, chunk, nj = dims
    g, s, t = lax.axis_index("grp"), lax.axis_index("sp"), lax.axis_index("tp")
    rows, width = resid_ref.shape
    tok, att_w = q_ref.shape
    depth, units = w_gate_ref.shape
    nheads = att_w // HEAD_DIM
    half_depth = depth // 2
    dup = ns * chunk - units
    nu, dj = chunk // UNIT, depth // nj
    wide = ns * dj
    x, c = t // 2, t % 2
    tx = (t + 2) % 4
    tc = t + 1 - 2 * c
    scale = HEAD_DIM ** (-0.5)
    sc = jax.named_scope

    def start_of(i):
        return min(i * chunk, units - chunk)

    def first_unit(i):
        return dup // UNIT if i == ns - 1 else 0

    def remote(src, dst, send, recv, **where):
        return pltpu.make_async_remote_copy(
            src_ref=src, dst_ref=dst, send_sem=send, recv_sem=recv, device_id=where,
            device_id_type=MESH,
        )

    def xor(a, b):
        hi, lo, bh, bl = a // 2, a % 2, b // 2, b % 2
        return 2 * (hi + bh - 2 * hi * bh) + lo + bl - 2 * lo * bl

    def on_each_s(body):
        for k in range(ns):
            pl.when(s == k)(lambda k=k: (body(k), None)[1])

    def each(low, high, body):
        lax.fori_loop(low, high, lambda i, z: (body(i), z)[1], 0)

    def unit_band(src, half):
        return pl.ds(pl.multiple_of(src * depth + half * half_depth, half_depth), half_depth)

    def unit_z(mat, u, me, dst):
        src = (w_gate_ref, w_up_ref)[mat].at[
            pl.ds(pl.multiple_of(g * half_depth, half_depth), half_depth),
            pl.ds(start_of(dst) + u * UNIT, UNIT),
        ]
        return remote(
            src, wgu.at[u, unit_band(me, g), pl.ds(mat * UNIT, UNIT)],
            wz_send.at[2 * u + mat, dst], wz_recv.at[2 * u + mat, me], sp=dst,
        )

    def unit_in(mat, u, src):
        block = wgu.at[u, unit_band(src, g), pl.ds(mat * UNIT, UNIT)]
        return remote(block, block, wz_send.at[2 * u + mat, src], wz_recv.at[2 * u + mat, src], sp=src)

    def unit_y(u, src, half):
        block = wgu.at[u, unit_band(src, half)]
        return remote(block, block, wy_send.at[u, src], wy_recv.at[u, src], grp=1 - g)

    def send_units(me, dst, us):
        for u in us:
            if u >= first_unit(dst):
                for mat in range(2):
                    unit_z(mat, u, me, dst).start()

    def pass_units(me, u, *srcs):
        if u >= first_unit(me):
            for src in srcs:
                for mat in range(2):
                    unit_in(mat, u, src).wait_recv()
                unit_y(u, src, g).start()

    def down_band(j, src, half, me):
        skip = first_unit(me) * UNIT
        size = (chunk - skip) // 2
        return wd.at[
            j, pl.ds(pl.multiple_of(skip + half * size, math.gcd(128, size)), size),
            pl.ds(src * dj, dj),
        ]

    def down_z(j, me, dst):
        skip = first_unit(dst) * UNIT
        size = (chunk - skip) // 2
        src = w_down_ref.at[
            pl.ds(pl.multiple_of(start_of(dst) + skip + g * size, math.gcd(128, size)), size),
            pl.ds(j * dj, dj),
        ]
        return remote(
            src, down_band(j, me, g, dst), dz_send.at[j, dst], dz_recv.at[j, me], sp=dst
        )

    def down_y(j, src, half, me):
        block = down_band(j, src, half, me)
        return remote(block, block, dy_send.at[j, src], dy_recv.at[j, src], grp=1 - g)

    def send_down(me, j, *dsts):
        for dst in dsts:
            down_z(j, me, dst).start()

    def pass_down(me, j, *srcs):
        for src in srcs:
            block = down_band(j, src, g, me)
            with sc(f"d{j}.{src}"):
                remote(block, block, dz_send.at[j, src], dz_recv.at[j, src], sp=src).wait_recv()
            down_y(j, src, g, me).start()

    barrier = pltpu.get_barrier_semaphore()

    def greet(i):
        pl.semaphore_signal(barrier, inc=1, device_id={"sp": i}, device_id_type=MESH)

    each(0, s, greet)
    each(s + 1, ns, greet)
    pl.semaphore_signal(barrier, inc=1, device_id={"grp": 1 - g}, device_id_type=MESH)
    for j in range(1, nt):
        pl.semaphore_signal(barrier, inc=1, device_id={"tp": (t + j) % nt}, device_id_type=MESH)
    with sc("bar"):
        pl.semaphore_wait(barrier, ns + nt - 1)

    def kv_out(i, kk, vv):
        return (
            remote(kk, kbuf.at[i], kv_send.at[0, i], kv_recv.at[0, i], sp=s + 1),
            remote(vv, vbuf.at[i], kv_send.at[1, i], kv_recv.at[1, i], sp=s + 1),
        )

    def kv_in(i):
        return (
            remote(kbuf.at[i], kbuf.at[i], kv_send.at[0, i], kv_recv.at[0, i], sp=s - 1),
            remote(vbuf.at[i], vbuf.at[i], kv_send.at[1, i], kv_recv.at[1, i], sp=s - 1),
        )

    @pl.when(s + 1 < ns)
    def _():
        for copy in kv_out(0, k_ref, v_ref):
            copy.start()

    w_out_copy = pltpu.make_async_copy(w_out_ref, w_out, loc_sem.at[0])
    w_out_copy.start()

    def locals_(me):
        own = pl.ds(me * depth, depth)
        copies = []
        for mat in range(2):
            for u in range(nu):
                copies.append(
                    pltpu.make_async_copy(
                        (w_gate_ref, w_up_ref)[mat].at[:, pl.ds(start_of(me) + u * UNIT, UNIT)],
                        wgu.at[u, own, pl.ds(mat * UNIT, UNIT)], loc_sem.at[1 + 2 * u + mat],
                    )
                )
        for j in range(nj):
            copies.append(
                pltpu.make_async_copy(
                    w_down_ref.at[pl.ds(start_of(me), chunk), pl.ds(j * dj, dj)],
                    wd.at[j, :, pl.ds(me * dj, dj)], loc_sem.at[1 + 2 * nu + j],
                )
            )
        return copies

    early = range(nu - 1)
    late = range(nu - 1, nu)

    def opening(me):
        for u in early:
            for dst in range(me - 1, -1, -1):
                send_units(me, dst, (u,))
        if me == 0:
            send_units(0, 1, range(nu))
        for copy in locals_(me):
            copy.start()

    on_each_s(opening)

    if dup:

        @pl.when(s == ns - 1)
        def _():
            for j in range(nj):
                wd[j, :dup, : (ns - 1) * dj] = jnp.zeros((dup, (ns - 1) * dj), BF16)
            for k in range(ns):
                hidden[k, :, :dup] = jnp.zeros((tok, dup), BF16)

    gate_own = gate_t_ref[:, pl.ds(pl.multiple_of(s * tok, tok), tok)].T

    def attend(src, kk, vv, first):
        for h in range(nheads):
            lanes = slice(h * HEAD_DIM, (h + 1) * HEAD_DIM)
            scores = lax.dot_general(
                q_ref[:, lanes], kk[:, lanes], (((1,), (1,)), ((), ())), preferred_element_type=F32
            )
            key_gate = gate_t_ref[h : h + 1, pl.ds(pl.multiple_of(src * tok, tok), tok)]
            scores = scores * scale + gate_own[:, h : h + 1] - key_gate
            if first:
                row = lax.broadcasted_iota(jnp.int32, (tok, tok), 0)
                col = lax.broadcasted_iota(jnp.int32, (tok, tok), 1)
                scores = jnp.where(col <= row, scores, -1e30)
                new = jnp.max(scores, axis=-1, keepdims=True)
                w = jnp.where(col <= row, jnp.exp(scores - new), 0.0)
                tot[h] = jnp.sum(w, axis=-1, keepdims=True)
                acc[h] = jnp.dot(w.astype(BF16), vv[:, lanes], preferred_element_type=F32)
            else:
                old = top[h]
                new = jnp.maximum(old, jnp.max(scores, axis=-1, keepdims=True))
                w = jnp.exp(scores - new)
                shrink = jnp.exp(old - new)
                tot[h] = tot[h] * shrink + jnp.sum(w, axis=-1, keepdims=True)
                acc[h] = acc[h] * shrink + jnp.dot(
                    w.astype(BF16), vv[:, lanes], preferred_element_type=F32
                )
            top[h] = new

    with sc("att0"):
        attend(s, k_ref, v_ref, True)

    def earlier(i):
        for copy in kv_in(i - 1):
            copy.wait_recv()

        @pl.when(s + 1 < ns)
        def _():
            for copy in kv_out(i, kbuf.at[i - 1], vbuf.at[i - 1]):
                copy.start()

        attend(s - i, kbuf.at[i - 1], vbuf.at[i - 1], False)

    with sc("earlier"):
        each(1, s + 1, earlier)

    for h in range(nheads):
        att[:, h * HEAD_DIM : (h + 1) * HEAD_DIM] = (acc[h] / tot[h]).astype(BF16)

    def head_copy(j):
        dst = (t + j) % nt
        return remote(
            att.at[pl.ds(pl.multiple_of(dst * rows, rows), rows)], heads.at[j - 1],
            h_send.at[j - 1], h_recv.at[j - 1], tp=dst,
        )

    for j in range(1, nt):
        head_copy(j).start()

    with sc("mix"):
        w_out_copy.wait()
        resid[...] = resid_ref[...].astype(F32) + jnp.dot(
            att[pl.ds(pl.multiple_of(t * rows, rows), rows), :],
            w_out[pl.ds(pl.multiple_of(t * att_w, att_w), att_w), :], preferred_element_type=F32,
        )

        def mix(j):
            head_copy(j).wait_recv()
            src = (t + nt - j) % nt
            resid[...] += jnp.dot(
                heads[j - 1], w_out[pl.ds(pl.multiple_of(src * att_w, att_w), att_w), :],
                preferred_element_type=F32,
            )

        each(1, nt, mix)
        full = resid[...]
        normed = full * lax.rsqrt(jnp.mean(full * full, axis=-1, keepdims=True) + 1e-06)
        nall[s, t] = (normed * gain_ref[...]).astype(BF16)

    def row_z(kind, src, to):
        block = nall.at[src, t]
        return remote(block, block, az_send.at[kind, src], az_recv.at[src], sp=to)

    def row_x(src, who):
        block = nall.at[src, who]
        return remote(block, block, ax_send.at[src], ax_recv.at[src], tp=tx)

    def row_c(kind, src, who):
        block = nall.at[src, who]
        return remote(block, block, ac_send.at[kind, src], ac_recv.at[kind, src], tp=tc)

    def spread(src):
        row_x(src, t).start()
        row_c(0, src, t).start()

    def relay(src):
        row_x(src, tx).wait_recv()
        row_c(1, src, tx).start()

    def take(me, src):
        row_z(0, src, me).wait_recv()
        if (me, src // 2) in ((1, 1), (2, 0)):
            row_z(0, src, me ^ 1).start()
        spread(src)

    def gather(me):
        near, mid = me ^ 1, 2 if me < 2 else 1
        row_z(1, me, mid).start()
        row_z(0, me, near).start()
        spread(me)
        last = nu - 1
        if me < 2:
            for u in range(nu):
                send_units(me, 2, (u,))
                send_units(me, 3, (u,))
        if me == 0:
            relay(0)
            for u in early:
                pass_units(0, u, 1, 2, 3)
            for u in late:
                pass_units(0, u, 1)
            take(0, 1)
            relay(1)
            for j in range(nj):
                send_down(0, j, 1)
            take(0, 2)
            take(0, 3)
            relay(2)
            for u in late:
                pass_units(0, u, 2, 3)
            relay(3)
            send_down(0, 0, 2, 3)
        elif me == 1:
            send_units(1, 0, late)
            for j in range(nj):
                send_down(1, j, 0)
            for u in range(nu):
                pass_units(1, u, 0)
            relay(1)
            for u in early:
                pass_units(1, u, 2, 3)
            take(1, 0)
            take(1, 2)
            take(1, 3)
            relay(0)
            pass_units(1, last, 2)
            relay(2)
            pass_units(1, last, 3)
            for j in range(nj):
                send_down(1, j, 2, 3)
            relay(3)
        elif me == 2:
            send_units(2, 1, late)
            send_units(2, 3, range(last))
            for u in early:
                pass_units(2, u, 3)
            relay(2)
            take(2, 0)
            take(2, 1)
            send_units(2, 3, late)
            pass_units(2, 0, 0)
            relay(0)
            pass_units(2, 1, 0)
            relay(1)
            for u in late:
                pass_units(2, u, 0, 3)
            send_units(2, 0, late)
            pass_units(2, 0, 1)
            take(2, 3)
            send_down(2, 0, 1)
            pass_units(2, 1, 1)
            relay(3)
            send_down(2, 0, 0, 3)
            for j in range(1, nj):
                send_down(2, j, 3)
        else:
            send_units(3, 2, late)
            send_units(3, 1, late)
            relay(3)
            take(3, 2)
            pass_units(3, 0, 2, 0)
            pass_units(3, 1, 2, 0)
            relay(2)
            take(3, 0)
            send_units(3, 0, late)
            pass_units(3, last, 0)
            for j in range(nj):
                send_down(3, j, 2)
            take(3, 1)
            relay(0)
            pass_units(3, 0, 1)
            pass_units(3, 1, 1)
            pass_units(3, last, 2)
            relay(1)
            send_down(3, 0, 1, 0)

    with sc("gather"):
        on_each_s(gather)

    def between(me, u):
        if u == 0:
            if me >= 2:
                for i in late:
                    pass_units(me, i, 1)
            elif me == 1:
                pass_down(1, 0, 0, 2)
            else:
                pass_down(0, 0, 1)
        elif u == 1:
            if me in (0, 2, 3):
                for j in range(1, nj):
                    send_down(me, j, *((2, 3) if me == 0 else (1, 0)))
            if me >= 2:
                pass_down(me, 0, me ^ 1, 1)
            else:
                pass_down(me, 0, 2 if me == 0 else 3)
        elif u == nu - 1:
            if me < 2:
                if me == 0:
                    pass_down(0, 0, 3)
            else:
                pass_down(me, 0, 0)

    def own_units(u):
        def body(me):
            copies = locals_(me)
            for mat in range(2):
                copies[mat * nu + u].wait()

        on_each_s(body)

    def own_down(j):
        on_each_s(lambda me: locals_(me)[2 * nu + j].wait())

    def twin_units(u):
        def body(me):
            if u >= first_unit(me):
                for src in range(ns):
                    if src != me:
                        unit_y(u, src, 1 - g).wait_recv()

        on_each_s(body)

    def twin_down(j):
        def body(me):
            for src in range(ns):
                if src != me:
                    down_y(j, src, 1 - g, me).wait_recv()

        on_each_s(body)

    def hide(u):
        def block(k):
            y = jnp.dot(nall[k].reshape(tok, width), wgu[u], preferred_element_type=F32)
            gate, up = y[:, :UNIT], y[:, UNIT:]
            hidden[k, :, u * UNIT : (u + 1) * UNIT] = (gate / (1.0 + jnp.exp(-gate)) * up).astype(BF16)

        def run():
            each(0, ns, block)

        if (u + 1) * UNIT <= dup:
            pl.when(s < ns - 1)(run)
        else:
            run()

    with sc("rows"):

        def rows_in(k):
            row_c(0, k, tc).wait_recv()
            row_c(1, k, (tc + 2) % 4).wait_recv()

        each(0, ns, rows_in)
    for u in range(nu):
        with sc(f"tw{u}"):
            own_units(u)
            twin_units(u)
        with sc(f"hide{u}"):
            hide(u)
        with sc(f"bt{u}"):
            on_each_s(lambda me, u=u: between(me, u))

    def pass_down_all(j):
        on_each_s(lambda me: pass_down(me, j, me ^ 1, me ^ 2, me ^ 3))

    steps = [(j, m) for j in range(nj) for m in (3, 1, 2, 0)]
    nd = len(steps)

    def sum_c(d):
        return remote(part.at[d, :, 1 - c], crecv.at[d], rc_send.at[d], rc_recv.at[d], tp=tc)

    def sum_x(d):
        return remote(csend.at[d], xrecv.at[d], rx_send.at[d], rx_recv.at[d], tp=tx)

    def sum_z(d):
        far = steps[d][1] == 2
        return remote(
            zsend.at[d], zrecv.at[d], rz_send.at[d], rz_recv.at[d], sp=xor(s, 2 if far else 1)
        )

    def stage_x(d):
        sum_c(d).wait_recv()
        csend[d] = (part[d, 1 - x, c].astype(F32) + crecv[d, 1 - x].astype(F32)).astype(BF16)
        sum_x(d).start()
        keep[d] = part[d, x, c].astype(F32) + crecv[d, x].astype(F32)

    def stage_z(d):
        m = steps[d][1]
        if m == 0:
            return
        sum_x(d).wait_recv()
        total = keep[d] + xrecv[d].astype(F32)
        if m == 2:
            sum_z(d - 2).wait_recv()
            total = total + zrecv[d - 2].astype(F32)
        zsend[d] = total.astype(BF16)
        sum_z(d).start()

    def feed(d):
        j, m = steps[d]
        src = hidden[xor(s, m)]
        piece = math.gcd(wide, 512)

        def down(p):
            cols = pl.ds(pl.multiple_of(p * piece, piece), piece)
            y = jnp.dot(src, wd[j, :, cols], preferred_element_type=F32).astype(BF16)
            part[d, :, :, :, cols] = y.reshape(2, 2, rows, piece)

        each(0, wide // piece, down)
        sum_c(d).start()

    def finish(j):
        d = 4 * j + 3
        sum_x(d).wait_recv()
        sum_z(d - 1).wait_recv()
        sum_z(d - 2).wait_recv()
        total = (
            keep[d] + xrecv[d].astype(F32) + zrecv[d - 1].astype(F32) + zrecv[d - 2].astype(F32)
        )
        for p in range(ns):
            cols = slice(p * depth + j * dj, p * depth + (j + 1) * dj)
            out_ref[:, cols] = (resid[:, cols] + total[:, p * dj : (p + 1) * dj]).astype(BF16)

    for d in range(nd):
        j, k = d // 4, d % 4
        if k == 0:
            with sc(f"td{j}"):
                own_down(j)
                twin_down(j)
        for ahead in range(1, nj):
            if d == 1 + (ahead - 1) * 5 // 2:
                with sc(f"pd{ahead}"):
                    pass_down_all(ahead)
        with sc(f"f{d}"):
            feed(d)
            if d >= 1:
                stage_x(d - 1)
            if d >= 3:
                stage_z(d - 3)
    with sc("st"):
        stage_x(nd - 1)
        for d in range(nd - 3, nd):
            stage_z(d)
    for j in range(nj):
        with sc(f"fin{j}"):
            finish(j)

    @pl.when(s + 1 < ns)
    def _():
        def sent(i):
            for copy in kv_out(i, kbuf.at[0], vbuf.at[0]):
                copy.wait_send()

        each(0, s + 1, sent)

    def drain(me):
        row_z(0, me, me ^ 1).wait_send()
        row_z(1, me, me ^ 1).wait_send()
        for src in range(ns):
            if (me, src // 2) in ((1, 1), (2, 0)):
                row_z(0, src, me ^ 1).wait_send()
            if src != me:
                for u in range(nu):
                    if u >= first_unit(src):
                        for mat in range(2):
                            unit_z(mat, u, me, src).wait_send()
                    if u >= first_unit(me):
                        unit_y(u, src, g).wait_send()
                for j in range(nj):
                    down_z(j, me, src).wait_send()
                    down_y(j, src, g, me).wait_send()

    with sc("drain"):
        on_each_s(drain)
        for j in range(1, nt):
            head_copy(j).wait_send()

        def spread_done(i):
            row_x(i, t).wait_send()
            row_c(0, i, t).wait_send()
            row_c(1, i, tx).wait_send()

        each(0, ns, spread_done)
        for d in range(nd):
            sum_c(d).wait_send()
            sum_x(d).wait_send()
            if steps[d][1]:
                sum_z(d).wait_send()


def fused(ns, nt, chunk, nj, resid_in, queries, keys, values, cum_gate, w_out, norm_gain, w_gate, w_up, w_down):
    rows, width = resid_in.shape
    tok, att_w = queries.shape
    depth, units = w_gate.shape
    nheads = att_w // HEAD_DIM
    nu, nd, wide = chunk // UNIT, 4 * nj, width // nj
    vm = pl.BlockSpec(memory_space=pltpu.VMEM)
    hbm = pl.BlockSpec(memory_space=pltpu.HBM)
    dma = pltpu.SemaphoreType.DMA
    return pl.pallas_call(
        functools.partial(layer_kernel, (ns, nt, chunk, nj)),
        out_shape=jax.ShapeDtypeStruct((rows, width), BF16),
        in_specs=[vm] * 6 + [hbm] * 4,
        out_specs=vm,
        scratch_shapes=[
            pltpu.VMEM((ns - 1, tok, att_w), BF16),
            pltpu.VMEM((ns - 1, tok, att_w), BF16),
            pltpu.VMEM((nheads, tok, 1), F32),
            pltpu.VMEM((nheads, tok, 1), F32),
            pltpu.VMEM((nheads, tok, HEAD_DIM), F32),
            pltpu.VMEM((tok, att_w), BF16),
            pltpu.VMEM((nt - 1, rows, att_w), BF16),
            pltpu.VMEM(w_out.shape, BF16),
            pltpu.VMEM((rows, width), F32),
            pltpu.VMEM((ns, nt, rows, width), BF16),
            pltpu.VMEM((nu, width, 2 * UNIT), BF16),
            pltpu.VMEM((nj, chunk, wide), BF16),
            pltpu.VMEM((ns, tok, chunk), BF16),
            pltpu.VMEM((nd, 2, 2, rows, wide), BF16),
            pltpu.VMEM((nd, 2, rows, wide), BF16),
            pltpu.VMEM((nd, rows, wide), BF16),
            pltpu.VMEM((nd, rows, wide), F32),
            pltpu.VMEM((nd, rows, wide), BF16),
            pltpu.VMEM((nd, rows, wide), BF16),
            pltpu.VMEM((nd, rows, wide), BF16),
            dma((1 + 2 * nu + nj,)),
            dma((2, ns)), dma((2, ns)),
            dma((2 * nu, ns)), dma((2 * nu, ns)),
            dma((nu, ns)), dma((nu, ns)),
            dma((nj, ns)), dma((nj, ns)),
            dma((nj, ns)), dma((nj, ns)),
            dma((nt - 1,)), dma((nt - 1,)),
            dma((2, ns)), dma((ns,)),
            dma((ns,)), dma((ns,)),
            dma((2, ns)), dma((2, ns)),
            dma((nd,)), dma((nd,)),
            dma((nd,)), dma((nd,)),
            dma((nd,)), dma((nd,)),
        ],
        compiler_params=pltpu.CompilerParams(
            collective_id=0, has_side_effects=True, vmem_limit_bytes=60 * 2**20
        ),
        name="layer",
    )(
        resid_in, queries, keys, values, cum_gate.T, norm_gain[None, :], w_out, w_gate,
        w_up, w_down,
    )


def pick(mesh):
    ng, ns, nt = (mesh.shape[a] for a in ("grp", "sp", "tp"))

    def step(*args):
        resid_in, queries, cum_gate, w_gate = args[0], args[1], args[4], args[7]
        rows, width = resid_in.shape
        depth, units = w_gate.shape
        chunk = -(-units // (128 * ns)) * 128
        need = 2 * ns * nt * rows * width * 4 + 6 * width * chunk + 2 * args[5].size
        fits = (
            ng == 2 and nt == 4 and ns == 4 and units % UNIT == 0 and chunk >= 2 * UNIT and depth % (128 * PIECES) == 0 and (ns - 1) * chunk < units
            and depth % 256 == 0 and width % 256 == 0 and (chunk - ns * chunk + units) % 32 == 0 and width == ns * depth and rows % 16 == 0
            and queries.shape[0] == rows * nt and queries.shape[0] % 128 == 0
            and cum_gate.shape[0] == ns * nt * rows and queries.shape[1] % 128 == 0
            and need < 40 * 2**20
        )
        if fits:
            return fused(ns, nt, chunk, PIECES, *args)
        return on_device(*args)

    return step


def solution(mesh):
    return jax.shard_map(
        pick(mesh),
        mesh=mesh,
        in_specs=(
            P(("grp", "sp", "tp"), None),
            P(("grp", "sp"), "tp"),
            P(("grp", "sp"), "tp"),
            P(("grp", "sp"), "tp"),
            P("grp", "tp"),
            P(),
            P(),
            P("sp", "tp"),
            P("sp", "tp"),
            P("tp", "sp"),
        ),
        out_specs=P(("grp", "sp", "tp"), None),
        check_vma=False,
    )
```

time: 119 us -> 110 us (0.924)
  Pallas kernels: 117 us -> 108 us
    pallas_call x1, Pallas kernels: 117 us -> 108 us  [fused(): pl.pallas_call(functools.partial(layer_kernel, (ns, nt, chunk, nj)), out_...]
where the time goes in v1:
time: 110 us
  Pallas kernels  108 us (98%)
  local copies, waits for them, and re-layouts  1.67 us (2%)
    pallas_call x1, Pallas kernels, fused(): pl.pallas_call(functools.partial(layer_kernel, (ns, nt, chunk, nj)), out_...  108 us

profile of v1, /device:TPU:0, one launch (start us, length us, event | category | flops | bytes accessed | tf_op | source)
XLA Modules:
  0.0 109.9 jit_solution(9167308801250260973)
XLA Ops:
  0.0 108.2 %layer.1 = bf16[64,2048]{1,0:T(8,128)(2,1)} custom-call(bf16[64,2048]{1,0:T(8,128)(2,1)} %resid_ref.1, bf16[256,256]{1,0:T(8,128)(2,1)} %q_ref.1, bf16[256,256]{1,0:T(8,128)(2,1)} %k_ref.1, bf16[256,256]{1,0:T(8,128)(2,1)} %v_ref.1, f32[4,1024]{1,0:T(4,128)} %bitcast.2, f32[1,2048]{1,0:T(1,128)} %bitcast.3, bf16[1024,2048]{1,0:T(8,128)(2,1)} %w_out_ref.1, ...), custom_call_target="tpu_custom_call" | custom-call | tf_op jit(solution)/shard_map/layer/pallas_call | solution.py:712
  108.2 1.7 %copy.12 = bf16[64,2048]{1,0:T(8,128)(2,1)} copy(bf16[64,2048]{1,0:T(8,128)(2,1)} %layer.1) | data formatting | bytes 524288

commit v2 on v1

--- a/solution.py
+++ b/solution.py
@@ -157,16 +157,16 @@
         ]
         return remote(
             src, wgu.at[u, unit_band(me, g), pl.ds(mat * UNIT, UNIT)],
-            wz_send.at[2 * u + mat, dst], wz_recv.at[2 * u + mat, me], sp=dst,
+            wz_send, wz_recv.at[2 * u + mat, me], sp=dst,
         )
 
     def unit_in(mat, u, src):
         block = wgu.at[u, unit_band(src, g), pl.ds(mat * UNIT, UNIT)]
-        return remote(block, block, wz_send.at[2 * u + mat, src], wz_recv.at[2 * u + mat, src], sp=src)
+        return remote(block, block, wz_send, wz_recv.at[2 * u + mat, src], sp=src)
 
     def unit_y(u, src, half):
         block = wgu.at[u, unit_band(src, half)]
-        return remote(block, block, wy_send.at[u, src], wy_recv.at[u, src], grp=1 - g)
+        return remote(block, block, wy_send, wy_recv.at[u, src], grp=1 - g)
 
     def send_units(me, dst, us):
         for u in us:
@@ -197,12 +197,12 @@
             pl.ds(j * dj, dj),
         ]
         return remote(
-            src, down_band(j, me, g, dst), dz_send.at[j, dst], dz_recv.at[j, me], sp=dst
+            src, down_band(j, me, g, dst), dz_send, dz_recv.at[j, me], sp=dst
         )
 
     def down_y(j, src, half, me):
         block = down_band(j, src, half, me)
-        return remote(block, block, dy_send.at[j, src], dy_recv.at[j, src], grp=1 - g)
+        return remote(block, block, dy_send, dy_recv.at[j, src], grp=1 - g)
 
     def send_down(me, j, *dsts):
         for dst in dsts:
@@ -212,7 +212,7 @@
         for src in srcs:
             block = down_band(j, src, g, me)
             with sc(f"d{j}.{src}"):
-                remote(block, block, dz_send.at[j, src], dz_recv.at[j, src], sp=src).wait_recv()
+                remote(block, block, dz_send, dz_recv.at[j, src], sp=src).wait_recv()
             down_y(j, src, g, me).start()
 
     barrier = pltpu.get_barrier_semaphore()
@@ -420,9 +420,10 @@
             take(0, 3)
             relay(2)
             for u in late:
-                pass_units(0, u, 2, 3)
+                pass_units(0, u, 2)
+            send_down(0, 0, 2, 3)
+            pass_down(0, 0, 1)
             relay(3)
-            send_down(0, 0, 2, 3)
         elif me == 1:
             send_units(1, 0, late)
             for j in range(nj):
@@ -449,19 +450,19 @@
                 pass_units(2, u, 3)
             relay(2)
             take(2, 0)
+            send_units(2, 3, late)
             take(2, 1)
-            send_units(2, 3, late)
             pass_units(2, 0, 0)
             relay(0)
             pass_units(2, 1, 0)
             relay(1)
             for u in late:
                 pass_units(2, u, 0, 3)
-            send_units(2, 0, late)
             pass_units(2, 0, 1)
             take(2, 3)
             send_down(2, 0, 1)
             pass_units(2, 1, 1)
+            send_units(2, 0, late)
             relay(3)
             send_down(2, 0, 0, 3)
             for j in range(1, nj):
@@ -475,44 +476,49 @@
             pass_units(3, 1, 2, 0)
             relay(2)
             take(3, 0)
-            send_units(3, 0, late)
+            send_down(3, 0, 1)
             pass_units(3, last, 0)
             for j in range(nj):
                 send_down(3, j, 2)
-            take(3, 1)
             relay(0)
             pass_units(3, 0, 1)
             pass_units(3, 1, 1)
+            send_units(3, 0, late)
+            send_down(3, 0, 0)
             pass_units(3, last, 2)
+            take(3, 1)
+            pass_units(3, last, 1)
             relay(1)
-            send_down(3, 0, 1, 0)
+            for j in range(1, nj):
+                send_down(3, j, 1, 0)
 
     with sc("gather"):
         on_each_s(gather)
 
     def between(me, u):
         if u == 0:
-            if me >= 2:
+            if me == 2:
                 for i in late:
-                    pass_units(me, i, 1)
+                    pass_units(2, i, 1)
+                pass_down(2, 0, 3)
+            elif me == 3:
+                pass_down(3, 0, 2, 1)
             elif me == 1:
                 pass_down(1, 0, 0, 2)
             else:
-                pass_down(0, 0, 1)
+                for i in late:
+                    pass_units(0, i, 3)
+                pass_down(0, 0, 2)
         elif u == 1:
-            if me in (0, 2, 3):
+            if me in (0, 2):
                 for j in range(1, nj):
                     send_down(me, j, *((2, 3) if me == 0 else (1, 0)))
-            if me >= 2:
-                pass_down(me, 0, me ^ 1, 1)
+            if me == 2:
+                pass_down(2, 0, 1, 0)
+            elif me == 3:
+                pass_down(3, 0, 0)
             else:
-                pass_down(me, 0, 2 if me == 0 else 3)
-        elif u == nu - 1:
-            if me < 2:
-                if me == 0:
-                    pass_down(0, 0, 3)
-            else:
-                pass_down(me, 0, 0)
+                pass_down(me, 0, 3)
 
     def own_units(u):
         def body(me):
@@ -575,20 +581,24 @@
     def pass_down_all(j):
         on_each_s(lambda me: pass_down(me, j, me ^ 1, me ^ 2, me ^ 3))
 
-    steps = [(j, m) for j in range(nj) for m in (3, 1, 2, 0)]
+    steps = [(0, m) for m in (3, 1, 2, 0)]
+    steps += [(j, m) for j in range(1, nj - 2) for m in (3, 1, 2)]
+    steps += [(j, m) for ms in ((3, 1), (2,)) for j in (nj - 2, nj - 1) for m in ms]
+    steps += [(j, 0) for j in range(1, nj)]
     nd = len(steps)
+    at = {step: d for d, step in enumerate(steps)}
+    slot = {d: i for i, d in enumerate(d for d in range(nd) if steps[d][1])}
 
     def sum_c(d):
-        return remote(part.at[d, :, 1 - c], crecv.at[d], rc_send.at[d], rc_recv.at[d], tp=tc)
+        return remote(part.at[d, :, 1 - c], crecv.at[d], rc_send, rc_recv.at[d], tp=tc)
 
     def sum_x(d):
-        return remote(csend.at[d], xrecv.at[d], rx_send.at[d], rx_recv.at[d], tp=tx)
+        return remote(csend.at[d], xrecv.at[d], rx_send, rx_recv.at[d], tp=tx)
 
     def sum_z(d):
-        far = steps[d][1] == 2
-        return remote(
-            zsend.at[d], zrecv.at[d], rz_send.at[d], rz_recv.at[d], sp=xor(s, 2 if far else 1)
-        )
+        i = slot[d]
+        to = xor(s, 2 if steps[d][1] == 2 else 1)
+        return remote(zsend.at[i], zrecv.at[i], rz_send, rz_recv.at[i], sp=to)
 
     def stage_x(d):
         sum_c(d).wait_recv()
@@ -597,15 +607,16 @@
         keep[d] = part[d, x, c].astype(F32) + crecv[d, x].astype(F32)
 
     def stage_z(d):
-        m = steps[d][1]
+        j, m = steps[d]
         if m == 0:
             return
         sum_x(d).wait_recv()
         total = keep[d] + xrecv[d].astype(F32)
         if m == 2:
-            sum_z(d - 2).wait_recv()
-            total = total + zrecv[d - 2].astype(F32)
-        zsend[d] = total.astype(BF16)
+            from_near = at[j, 3]
+            sum_z(from_near).wait_recv()
+            total = total + zrecv[slot[from_near]].astype(F32)
+        zsend[slot[d]] = total.astype(BF16)
         sum_z(d).start()
 
     def feed(d):
@@ -622,33 +633,36 @@
         sum_c(d).start()
 
     def finish(j):
-        d = 4 * j + 3
+        d, near, far = at[j, 0], at[j, 1], at[j, 2]
         sum_x(d).wait_recv()
-        sum_z(d - 1).wait_recv()
-        sum_z(d - 2).wait_recv()
+        sum_z(near).wait_recv()
+        sum_z(far).wait_recv()
         total = (
-            keep[d] + xrecv[d].astype(F32) + zrecv[d - 1].astype(F32) + zrecv[d - 2].astype(F32)
+            keep[d] + xrecv[d].astype(F32) + zrecv[slot[near]].astype(F32)
+            + zrecv[slot[far]].astype(F32)
         )
         for p in range(ns):
             cols = slice(p * depth + j * dj, p * depth + (j + 1) * dj)
             out_ref[:, cols] = (resid[:, cols] + total[:, p * dj : (p + 1) * dj]).astype(BF16)
 
+    ready = set()
     for d in range(nd):
-        j, k = d // 4, d % 4
-        if k == 0:
+        j = steps[d][0]
+        if j not in ready:
+            ready.add(j)
             with sc(f"td{j}"):
                 own_down(j)
                 twin_down(j)
-        for ahead in range(1, nj):
-            if d == 1 + (ahead - 1) * 5 // 2:
-                with sc(f"pd{ahead}"):
-                    pass_down_all(ahead)
         with sc(f"f{d}"):
             feed(d)
             if d >= 1:
                 stage_x(d - 1)
             if d >= 3:
                 stage_z(d - 3)
+        for ahead in range(1, nj):
+            if d == 2 * ahead - 1:
+                with sc(f"pd{ahead}"):
+                    pass_down_all(ahead)
     with sc("st"):
         stage_x(nd - 1)
         for d in range(nd - 3, nd):
@@ -671,16 +685,20 @@
         for src in range(ns):
             if (me, src // 2) in ((1, 1), (2, 0)):
                 row_z(0, src, me ^ 1).wait_send()
-            if src != me:
-                for u in range(nu):
-                    if u >= first_unit(src):
-                        for mat in range(2):
-                            unit_z(mat, u, me, src).wait_send()
-                    if u >= first_unit(me):
-                        unit_y(u, src, g).wait_send()
-                for j in range(nj):
-                    down_z(j, me, src).wait_send()
-                    down_y(j, src, g, me).wait_send()
+        others = [i for i in range(ns) if i != me]
+        for count, sem in (
+            (sum(nu - first_unit(i) for i in others), wz_send),
+            ((ns - 1) * (nu - first_unit(me)), wy_send),
+        ):
+            high = count * half_depth
+            all_of = wgu.at[0, :high] if high <= width else wgu.at[:, : high // nu]
+            remote(all_of, all_of, sem, wz_recv.at[0, me], grp=1 - g).wait_send()
+        halves = [(chunk - first_unit(i) * UNIT) // 2 for i in range(ns)]
+        for count, sem in (
+            (sum(halves[i] for i in others), dz_send), ((ns - 1) * halves[me], dy_send)
+        ):
+            all_of = wd.at[:, : count // ns]
+            remote(all_of, all_of, sem, dz_recv.at[0, me], grp=1 - g).wait_send()
 
     with sc("drain"):
         on_each_s(drain)
@@ -693,11 +711,9 @@
             row_c(1, i, tx).wait_send()
 
         each(0, ns, spread_done)
-        for d in range(nd):
-            sum_c(d).wait_send()
-            sum_x(d).wait_send()
-            if steps[d][1]:
-                sum_z(d).wait_send()
+        remote(crecv, crecv, rc_send, rc_recv.at[0], tp=tc).wait_send()
+        remote(xrecv, xrecv, rx_send, rx_recv.at[0], tp=tx).wait_send()
+        remote(zrecv, zrecv, rz_send, rz_recv.at[0], tp=tx).wait_send()
 
 
 def fused(ns, nt, chunk, nj, resid_in, queries, keys, values, cum_gate, w_out, norm_gain, w_gate, w_up, w_down):
@@ -733,21 +749,21 @@
             pltpu.VMEM((nd, rows, wide), BF16),
             pltpu.VMEM((nd, rows, wide), F32),
             pltpu.VMEM((nd, rows, wide), BF16),
-            pltpu.VMEM((nd, rows, wide), BF16),
-            pltpu.VMEM((nd, rows, wide), BF16),
+            pltpu.VMEM((3 * nj, rows, wide), BF16),
+            pltpu.VMEM((3 * nj, rows, wide), BF16),
             dma((1 + 2 * nu + nj,)),
             dma((2, ns)), dma((2, ns)),
-            dma((2 * nu, ns)), dma((2 * nu, ns)),
-            dma((nu, ns)), dma((nu, ns)),
-            dma((nj, ns)), dma((nj, ns)),
-            dma((nj, ns)), dma((nj, ns)),
+            dma, dma((2 * nu, ns)),
+            dma, dma((nu, ns)),
+            dma, dma((nj, ns)),
+            dma, dma((nj, ns)),
             dma((nt - 1,)), dma((nt - 1,)),
             dma((2, ns)), dma((ns,)),
             dma((ns,)), dma((ns,)),
             dma((2, ns)), dma((2, ns)),
-            dma((nd,)), dma((nd,)),
-            dma((nd,)), dma((nd,)),
-            dma((nd,)), dma((nd,)),
+            dma, dma((nd,)),
+            dma, dma((nd,)),
+            dma, dma((3 * nj,)),
         ],
         compiler_params=pltpu.CompilerParams(
             collective_id=0, has_side_effects=True, vmem_limit_bytes=60 * 2**20

time: 110 us -> 106 us (0.964)
  Pallas kernels: 108 us -> 104 us
    pallas_call x1, Pallas kernels: 108 us -> 104 us  [fused(): pl.pallas_call(functools.partial(layer_kernel, (ns, nt, chunk, nj)), out_...]
where the time goes in v2:
time: 106 us
  Pallas kernels  104 us (98%)
  local copies, waits for them, and re-layouts  1.67 us (2%)
    pallas_call x1, Pallas kernels, fused(): pl.pallas_call(functools.partial(layer_kernel, (ns, nt, chunk, nj)), out_...  104 us

profile of v2, /device:TPU:0, one launch (start us, length us, event | category | flops | bytes accessed | tf_op | source)
XLA Modules:
  0.0 105.9 jit_solution(3227234437714841964)
XLA Ops:
  0.0 104.2 %layer.1 = bf16[64,2048]{1,0:T(8,128)(2,1)} custom-call(bf16[64,2048]{1,0:T(8,128)(2,1)} %resid_ref.1, bf16[256,256]{1,0:T(8,128)(2,1)} %q_ref.1, bf16[256,256]{1,0:T(8,128)(2,1)} %k_ref.1, bf16[256,256]{1,0:T(8,128)(2,1)} %v_ref.1, f32[4,1024]{1,0:T(4,128)} %bitcast.2, f32[1,2048]{1,0:T(1,128)} %bitcast.3, bf16[1024,2048]{1,0:T(8,128)(2,1)} %w_out_ref.1, ...), custom_call_target="tpu_custom_call" | custom-call | tf_op jit(solution)/shard_map/layer/pallas_call | solution.py:728
  104.2 1.7 %copy.12 = bf16[64,2048]{1,0:T(8,128)(2,1)} copy(bf16[64,2048]{1,0:T(8,128)(2,1)} %layer.1) | data formatting | bytes 524288

commit v3 on v2

--- a/solution.py
+++ b/solution.py
@@ -157,16 +157,16 @@
         ]
         return remote(
             src, wgu.at[u, unit_band(me, g), pl.ds(mat * UNIT, UNIT)],
-            wz_send, wz_recv.at[2 * u + mat, me], sp=dst,
+            wz_send, wz_recv.at[u, me], sp=dst,
         )
 
-    def unit_in(mat, u, src):
-        block = wgu.at[u, unit_band(src, g), pl.ds(mat * UNIT, UNIT)]
-        return remote(block, block, wz_send, wz_recv.at[2 * u + mat, src], sp=src)
+    def unit_in(u, src):
+        block = wgu.at[u, unit_band(src, g)]
+        return remote(block, block, wz_send, wz_recv.at[u, src], sp=src)
 
     def unit_y(u, src, half):
         block = wgu.at[u, unit_band(src, half)]
-        return remote(block, block, wy_send, wy_recv.at[u, src], grp=1 - g)
+        return remote(block, block, wy_send, wy_recv.at[u], grp=1 - g)
 
     def send_units(me, dst, us):
         for u in us:
@@ -177,8 +177,8 @@
     def pass_units(me, u, *srcs):
         if u >= first_unit(me):
             for src in srcs:
-                for mat in range(2):
-                    unit_in(mat, u, src).wait_recv()
+                with sc(f"y{u}.{src}"):
+                    unit_in(u, src).wait_recv()
                 unit_y(u, src, g).start()
 
     def down_band(j, src, half, me):
@@ -202,7 +202,7 @@
 
     def down_y(j, src, half, me):
         block = down_band(j, src, half, me)
-        return remote(block, block, dy_send, dy_recv.at[j, src], grp=1 - g)
+        return remote(block, block, dy_send, dy_recv.at[j], grp=1 - g)
 
     def send_down(me, j, *dsts):
         for dst in dsts:
@@ -230,14 +230,14 @@
 
     def kv_out(i, kk, vv):
         return (
-            remote(kk, kbuf.at[i], kv_send.at[0, i], kv_recv.at[0, i], sp=s + 1),
-            remote(vv, vbuf.at[i], kv_send.at[1, i], kv_recv.at[1, i], sp=s + 1),
+            remote(kk, kbuf.at[i], kv_send.at[0], kv_recv.at[0, i], sp=s + 1),
+            remote(vv, vbuf.at[i], kv_send.at[1], kv_recv.at[1, i], sp=s + 1),
         )
 
     def kv_in(i):
         return (
-            remote(kbuf.at[i], kbuf.at[i], kv_send.at[0, i], kv_recv.at[0, i], sp=s - 1),
-            remote(vbuf.at[i], vbuf.at[i], kv_send.at[1, i], kv_recv.at[1, i], sp=s - 1),
+            remote(kbuf.at[i], kbuf.at[i], kv_send.at[0], kv_recv.at[0, i], sp=s - 1),
+            remote(vbuf.at[i], vbuf.at[i], kv_send.at[1], kv_recv.at[1, i], sp=s - 1),
         )
 
     @pl.when(s + 1 < ns)
@@ -274,7 +274,8 @@
     def opening(me):
         for u in early:
             for dst in range(me - 1, -1, -1):
-                send_units(me, dst, (u,))
+                if u == 0 or dst != 1:
+                    send_units(me, dst, (u,))
         if me == 0:
             send_units(0, 1, range(nu))
         for copy in locals_(me):
@@ -344,7 +345,7 @@
         dst = (t + j) % nt
         return remote(
             att.at[pl.ds(pl.multiple_of(dst * rows, rows), rows)], heads.at[j - 1],
-            h_send.at[j - 1], h_recv.at[j - 1], tp=dst,
+            h_send, h_recv.at[j - 1], tp=dst,
         )
 
     for j in range(1, nt):
@@ -370,37 +371,47 @@
         normed = full * lax.rsqrt(jnp.mean(full * full, axis=-1, keepdims=True) + 1e-06)
         nall[s, t] = (normed * gain_ref[...]).astype(BF16)
 
-    def row_z(kind, src, to):
-        block = nall.at[src, t]
-        return remote(block, block, az_send.at[kind, src], az_recv.at[src], sp=to)
-
-    def row_x(src, who):
-        block = nall.at[src, who]
-        return remote(block, block, ax_send.at[src], ax_recv.at[src], tp=tx)
-
-    def row_c(kind, src, who):
-        block = nall.at[src, who]
-        return remote(block, block, ac_send.at[kind, src], ac_recv.at[kind, src], tp=tc)
-
-    def spread(src):
-        row_x(src, t).start()
-        row_c(0, src, t).start()
+    part_rows = rows // 2
+
+    def half_of(src, who, h):
+        return nall.at[src, who, pl.ds(h * part_rows, part_rows)]
+
+    def row_z(src, to, h):
+        block = half_of(src, t, h)
+        return remote(block, block, az_send, az_recv.at[src, h], sp=to)
+
+    def row_x(src, who, h):
+        block = half_of(src, who, h)
+        return remote(block, block, ax_send, ax_recv.at[src, h], tp=tx)
+
+    def row_c(kind, src, who, h):
+        block = half_of(src, who, h)
+        return remote(block, block, ac_send, ac_recv.at[kind, src, h], tp=tc)
+
+    def spread(src, h):
+        row_x(src, t, h).start()
+        row_c(0, src, t, h).start()
 
     def relay(src):
-        row_x(src, tx).wait_recv()
-        row_c(1, src, tx).start()
+        for h in range(2):
+            row_x(src, tx, h).wait_recv()
+            row_c(1, src, tx, h).start()
 
     def take(me, src):
-        row_z(0, src, me).wait_recv()
-        if (me, src // 2) in ((1, 1), (2, 0)):
-            row_z(0, src, me ^ 1).start()
-        spread(src)
+        for h in range(2):
+            with sc(f"take{src}.{h}"):
+                row_z(src, me, h).wait_recv()
+            if (me, src // 2) in ((1, 1), (2, 0)):
+                row_z(src, me ^ 1, h).start()
+            spread(src, h)
 
     def gather(me):
         near, mid = me ^ 1, 2 if me < 2 else 1
-        row_z(1, me, mid).start()
-        row_z(0, me, near).start()
-        spread(me)
+        for h in range(2):
+            row_z(me, mid, h).start()
+        for h in range(2):
+            row_z(me, near, h).start()
+            spread(me, h)
         last = nu - 1
         if me < 2:
             for u in range(nu):
@@ -417,13 +428,13 @@
             for j in range(nj):
                 send_down(0, j, 1)
             take(0, 2)
+            for u in late:
+                pass_units(0, u, 2, 3)
             take(0, 3)
             relay(2)
-            for u in late:
-                pass_units(0, u, 2)
-            send_down(0, 0, 2, 3)
             pass_down(0, 0, 1)
             relay(3)
+            send_down(0, 0, 2, 3)
         elif me == 1:
             send_units(1, 0, late)
             for j in range(nj):
@@ -431,20 +442,21 @@
             for u in range(nu):
                 pass_units(1, u, 0)
             relay(1)
-            for u in early:
-                pass_units(1, u, 2, 3)
+            pass_units(1, 0, 2, 3)
             take(1, 0)
             take(1, 2)
+            relay(0)
             take(1, 3)
-            relay(0)
-            pass_units(1, last, 2)
             relay(2)
-            pass_units(1, last, 3)
             for j in range(nj):
                 send_down(1, j, 2, 3)
+            pass_units(1, 1, 2)
             relay(3)
+            pass_units(1, 1, 3)
+            for u in range(2, nu):
+                pass_units(1, u, 2, 3)
         elif me == 2:
-            send_units(2, 1, late)
+            send_units(2, 0, late)
             send_units(2, 3, range(last))
             for u in early:
                 pass_units(2, u, 3)
@@ -454,43 +466,42 @@
             take(2, 1)
             pass_units(2, 0, 0)
             relay(0)
+            send_units(2, 1, range(1, nu))
             pass_units(2, 1, 0)
             relay(1)
             for u in late:
                 pass_units(2, u, 0, 3)
             pass_units(2, 0, 1)
             take(2, 3)
-            send_down(2, 0, 1)
+            send_down(2, 0, 0, 1)
             pass_units(2, 1, 1)
-            send_units(2, 0, late)
             relay(3)
-            send_down(2, 0, 0, 3)
+            send_down(2, 0, 3)
             for j in range(1, nj):
                 send_down(2, j, 3)
         else:
             send_units(3, 2, late)
-            send_units(3, 1, late)
+            send_units(3, 0, late)
             relay(3)
             take(3, 2)
             pass_units(3, 0, 2, 0)
             pass_units(3, 1, 2, 0)
             relay(2)
+            send_units(3, 1, range(1, nu))
             take(3, 0)
-            send_down(3, 0, 1)
             pass_units(3, last, 0)
+            send_down(3, 0, 0, 1)
             for j in range(nj):
                 send_down(3, j, 2)
             relay(0)
             pass_units(3, 0, 1)
             pass_units(3, 1, 1)
-            send_units(3, 0, late)
-            send_down(3, 0, 0)
             pass_units(3, last, 2)
             take(3, 1)
             pass_units(3, last, 1)
             relay(1)
             for j in range(1, nj):
-                send_down(3, j, 1, 0)
+                send_down(3, j, 0, 1)
 
     with sc("gather"):
         on_each_s(gather)
@@ -504,21 +515,23 @@
             elif me == 3:
                 pass_down(3, 0, 2, 1)
             elif me == 1:
-                pass_down(1, 0, 0, 2)
+                pass_down(1, 0, 0)
             else:
-                for i in late:
-                    pass_units(0, i, 3)
                 pass_down(0, 0, 2)
         elif u == 1:
-            if me in (0, 2):
+            if me == 2:
                 for j in range(1, nj):
-                    send_down(me, j, *((2, 3) if me == 0 else (1, 0)))
-            if me == 2:
+                    send_down(2, j, 0, 1)
                 pass_down(2, 0, 1, 0)
             elif me == 3:
                 pass_down(3, 0, 0)
+            elif me == 1:
+                pass_down(1, 0, 2, 3)
             else:
-                pass_down(me, 0, 3)
+                pass_down(0, 0, 3)
+        elif u == nu - 1 and me == 0:
+            for j in range(1, nj):
+                send_down(0, j, 2, 3)
 
     def own_units(u):
         def body(me):
@@ -534,56 +547,63 @@
     def twin_units(u):
         def body(me):
             if u >= first_unit(me):
-                for src in range(ns):
-                    if src != me:
-                        unit_y(u, src, 1 - g).wait_recv()
+                all_of = wgu.at[u, : (ns - 1) * half_depth]
+                remote(all_of, all_of, wy_send, wy_recv.at[u], grp=1 - g).wait_recv()
 
         on_each_s(body)
 
     def twin_down(j):
         def body(me):
-            for src in range(ns):
-                if src != me:
-                    down_y(j, src, 1 - g, me).wait_recv()
+            all_of = wd.at[j, : (ns - 1) * ((chunk - first_unit(me) * UNIT) // 2) // ns]
+            remote(all_of, all_of, dy_send, dy_recv.at[j], grp=1 - g).wait_recv()
 
         on_each_s(body)
 
-    def hide(u):
-        def block(k):
+    final = ns - 1 - 2 * (s // (ns - 1))
+
+    def hide(u, low, high):
+        def block(i):
+            k = jnp.where(i == ns - 1, final, i + jnp.where(i >= final, 1, 0))
             y = jnp.dot(nall[k].reshape(tok, width), wgu[u], preferred_element_type=F32)
             gate, up = y[:, :UNIT], y[:, UNIT:]
             hidden[k, :, u * UNIT : (u + 1) * UNIT] = (gate / (1.0 + jnp.exp(-gate)) * up).astype(BF16)
 
         def run():
-            each(0, ns, block)
+            each(low, high, block)
 
         if (u + 1) * UNIT <= dup:
             pl.when(s < ns - 1)(run)
         else:
             run()
 
+    def rows_in(i):
+        k = jnp.where(i == ns - 1, final, i + jnp.where(i >= final, 1, 0))
+        for h in range(2):
+            row_c(0, k, tc, h).wait_recv()
+            row_c(1, k, (tc + 2) % 4, h).wait_recv()
+
     with sc("rows"):
-
-        def rows_in(k):
-            row_c(0, k, tc).wait_recv()
-            row_c(1, k, (tc + 2) % 4).wait_recv()
-
-        each(0, ns, rows_in)
+        each(0, ns - 1, rows_in)
     for u in range(nu):
         with sc(f"tw{u}"):
             own_units(u)
             twin_units(u)
         with sc(f"hide{u}"):
-            hide(u)
+            hide(u, 0, ns - 1)
         with sc(f"bt{u}"):
             on_each_s(lambda me, u=u: between(me, u))
+    with sc("rowl"):
+        rows_in(ns - 1)
+    with sc("hidel"):
+        for u in range(nu):
+            hide(u, ns - 1, ns)
 
     def pass_down_all(j):
         on_each_s(lambda me: pass_down(me, j, me ^ 1, me ^ 2, me ^ 3))
 
     steps = [(0, m) for m in (3, 1, 2, 0)]
     steps += [(j, m) for j in range(1, nj - 2) for m in (3, 1, 2)]
-    steps += [(j, m) for ms in ((3, 1), (2,)) for j in (nj - 2, nj - 1) for m in ms]
+    steps += [(j, m) for m in (3, 2, 1) for j in (nj - 2, nj - 1)]
     steps += [(j, 0) for j in range(1, nj)]
     nd = len(steps)
     at = {step: d for d, step in enumerate(steps)}
@@ -657,12 +677,12 @@
             feed(d)
             if d >= 1:
                 stage_x(d - 1)
-            if d >= 3:
+        if 2 <= d <= nj:
+            with sc(f"pd{d - 1}"):
+                pass_down_all(d - 1)
+        if d >= 3:
+            with sc(f"z{d}"):
                 stage_z(d - 3)
-        for ahead in range(1, nj):
-            if d == 2 * ahead - 1:
-                with sc(f"pd{ahead}"):
-                    pass_down_all(ahead)
     with sc("st"):
         stage_x(nd - 1)
         for d in range(nd - 3, nd):
@@ -671,20 +691,13 @@
         with sc(f"fin{j}"):
             finish(j)
 
-    @pl.when(s + 1 < ns)
-    def _():
-        def sent(i):
-            for copy in kv_out(i, kbuf.at[0], vbuf.at[0]):
-                copy.wait_send()
-
-        each(0, s + 1, sent)
-
     def drain(me):
-        row_z(0, me, me ^ 1).wait_send()
-        row_z(1, me, me ^ 1).wait_send()
-        for src in range(ns):
-            if (me, src // 2) in ((1, 1), (2, 0)):
-                row_z(0, src, me ^ 1).wait_send()
+        if me + 1 < ns:
+            for kind, buf in enumerate((kbuf, vbuf)):
+                sent = buf.at[: me + 1]
+                remote(sent, sent, kv_send.at[kind], kv_recv.at[kind, 0], tp=tx).wait_send()
+        sent = nall.at[0, : 2 if me in (0, ns - 1) else 4]
+        remote(sent, sent, az_send, az_recv.at[0, 0], tp=tx).wait_send()
         others = [i for i in range(ns) if i != me]
         for count, sem in (
             (sum(nu - first_unit(i) for i in others), wz_send),
@@ -702,15 +715,11 @@
 
     with sc("drain"):
         on_each_s(drain)
-        for j in range(1, nt):
-            head_copy(j).wait_send()
-
-        def spread_done(i):
-            row_x(i, t).wait_send()
-            row_c(0, i, t).wait_send()
-            row_c(1, i, tx).wait_send()
-
-        each(0, ns, spread_done)
+        remote(heads, heads, h_send, h_recv.at[0], tp=tx).wait_send()
+
+        remote(nall.at[0], nall.at[0], ax_send, ax_recv.at[0, 0], tp=tx).wait_send()
+        sent = nall.at[pl.ds(0, 2)]
+        remote(sent, sent, ac_send, ac_recv.at[0, 0, 0], tp=tx).wait_send()
         remote(crecv, crecv, rc_send, rc_recv.at[0], tp=tc).wait_send()
         remote(xrecv, xrecv, rx_send, rx_recv.at[0], tp=tx).wait_send()
         remote(zrecv, zrecv, rz_send, rz_recv.at[0], tp=tx).wait_send()
@@ -752,15 +761,15 @@
             pltpu.VMEM((3 * nj, rows, wide), BF16),
             pltpu.VMEM((3 * nj, rows, wide), BF16),
             dma((1 + 2 * nu + nj,)),
-            dma((2, ns)), dma((2, ns)),
-            dma, dma((2 * nu, ns)),
+            dma((2,)), dma((2, ns - 1)),
             dma, dma((nu, ns)),
+            dma, dma((nu,)),
             dma, dma((nj, ns)),
-            dma, dma((nj, ns)),
-            dma((nt - 1,)), dma((nt - 1,)),
-            dma((2, ns)), dma((ns,)),
-            dma((ns,)), dma((ns,)),
-            dma((2, ns)), dma((2, ns)),
+            dma, dma((nj,)),
+            dma, dma((nt - 1,)),
+            dma, dma((ns, 2)),
+            dma, dma((ns, 2)),
+            dma, dma((2, ns, 2)),
             dma, dma((nd,)),
             dma, dma((nd,)),
             dma, dma((3 * nj,)),
@@ -786,7 +795,7 @@
         need = 2 * ns * nt * rows * width * 4 + 6 * width * chunk + 2 * args[5].size
         fits = (
             ng == 2 and nt == 4 and ns == 4 and units % UNIT == 0 and chunk >= 2 * UNIT and depth % (128 * PIECES) == 0 and (ns - 1) * chunk < units
-            and depth % 256 == 0 and width % 256 == 0 and (chunk - ns * chunk + units) % 32 == 0 and width == ns * depth and rows % 16 == 0
+            and depth % 256 == 0 and width % 256 == 0 and (chunk - ns * chunk + units) % 32 == 0 and width == ns * depth and rows % 32 == 0
             and queries.shape[0] == rows * nt and queries.shape[0] % 128 == 0
             and cum_gate.shape[0] == ns * nt * rows and queries.shape[1] % 128 == 0
             and need < 40 * 2**20

time: 106 us -> 102 us (0.962)
  Pallas kernels: 104 us -> 100 us
    pallas_call x1, Pallas kernels: 104 us -> 100 us  [fused(): pl.pallas_call(functools.partial(layer_kernel, (ns, nt, chunk, nj)), out_...]
where the time goes in v3:
time: 102 us
  Pallas kernels  100 us (98%)
  local copies, waits for them, and re-layouts  1.67 us (2%)
    pallas_call x1, Pallas kernels, fused(): pl.pallas_call(functools.partial(layer_kernel, (ns, nt, chunk, nj)), out_...  100 us

profile of v3, /device:TPU:0, one launch (start us, length us, event | category | flops | bytes accessed | tf_op | source)
XLA Modules:
  0.0 102.0 jit_solution(3629458913229191735)
XLA Ops:
  0.0 100.3 %layer.1 = bf16[64,2048]{1,0:T(8,128)(2,1)} custom-call(bf16[64,2048]{1,0:T(8,128)(2,1)} %resid_ref.1, bf16[256,256]{1,0:T(8,128)(2,1)} %q_ref.1, bf16[256,256]{1,0:T(8,128)(2,1)} %k_ref.1, bf16[256,256]{1,0:T(8,128)(2,1)} %v_ref.1, f32[4,1024]{1,0:T(4,128)} %bitcast.2, f32[1,2048]{1,0:T(1,128)} %bitcast.3, bf16[1024,2048]{1,0:T(8,128)(2,1)} %w_out_ref.1, ...), custom_call_target="tpu_custom_call" | custom-call | tf_op jit(solution)/shard_map/layer/pallas_call | solution.py:737
  100.3 1.7 %copy.12 = bf16[64,2048]{1,0:T(8,128)(2,1)} copy(bf16[64,2048]{1,0:T(8,128)(2,1)} %layer.1) | data formatting | bytes 524288

commit v4 on v3

--- a/solution.py
+++ b/solution.py
@@ -102,16 +102,17 @@
 
 
 def layer_kernel(
-    dims, resid_ref, q_ref, k_ref, v_ref, gate_t_ref, gain_ref, w_out_ref, w_gate_ref,
-    w_up_ref, w_down_ref, out_ref, kbuf, vbuf, top, tot, acc, att, heads, w_out, resid, nall, wgu,
-    wd, hidden, part, crecv, csend, keep, xrecv, zsend, zrecv, loc_sem, kv_send, kv_recv, wz_send,
+    dims, resid_hbm, q_hbm, k_hbm, v_hbm, gate_t_hbm, gain_hbm, w_out_ref, w_gate_ref,
+    w_up_ref, w_down_ref, out_ref, resid_ref, q_ref, k_ref, v_ref, gate_t_ref, gain_ref, kbuf, vbuf, top, tot, acc, att, heads, w_out, resid, nall, wgu,
+    wd, hidden, part, crecv, csend, keep, xrecv, zsend, zrecv, frecv, in_sem, loc_sem, kv_send, kv_recv, wz_send,
     wz_recv, wy_send, wy_recv, dz_send, dz_recv, dy_send, dy_recv, h_send, h_recv, az_send, az_recv,
     ax_send, ax_recv, ac_send, ac_recv, rc_send, rc_recv, rx_send, rx_recv, rz_send, rz_recv,
+    rf_recv,
 ):
     ns, nt, chunk, nj = dims
     g, s, t = lax.axis_index("grp"), lax.axis_index("sp"), lax.axis_index("tp")
-    rows, width = resid_ref.shape
-    tok, att_w = q_ref.shape
+    rows, width = resid_hbm.shape
+    tok, att_w = q_hbm.shape
     depth, units = w_gate_ref.shape
     nheads = att_w // HEAD_DIM
     half_depth = depth // 2
@@ -157,15 +158,20 @@
         ]
         return remote(
             src, wgu.at[u, unit_band(me, g), pl.ds(mat * UNIT, UNIT)],
-            wz_send, wz_recv.at[u, me], sp=dst,
+            wz_send, wz_recv.at[u + (mat if u == nu - 1 else 0), me], sp=dst,
         )
 
-    def unit_in(u, src):
-        block = wgu.at[u, unit_band(src, g)]
-        return remote(block, block, wz_send, wz_recv.at[u, src], sp=src)
-
-    def unit_y(u, src, half):
-        block = wgu.at[u, unit_band(src, half)]
+    def unit_parts(u):
+        return ((0, 0, UNIT), (1, UNIT, UNIT)) if u == nu - 1 else ((0, 0, 2 * UNIT),)
+
+    def unit_in(u, src, part):
+        i, low, size = part
+        block = wgu.at[u, unit_band(src, g), pl.ds(low, size)]
+        return remote(block, block, wz_send, wz_recv.at[u + i, src], sp=src)
+
+    def unit_y(u, src, part):
+        _, low, size = part
+        block = wgu.at[u, unit_band(src, g), pl.ds(low, size)]
         return remote(block, block, wy_send, wy_recv.at[u], grp=1 - g)
 
     def send_units(me, dst, us):
@@ -178,8 +184,9 @@
         if u >= first_unit(me):
             for src in srcs:
                 with sc(f"y{u}.{src}"):
-                    unit_in(u, src).wait_recv()
-                unit_y(u, src, g).start()
+                    for part in unit_parts(u):
+                        unit_in(u, src, part).wait_recv()
+                        unit_y(u, src, part).start()
 
     def down_band(j, src, half, me):
         skip = first_unit(me) * UNIT
@@ -215,6 +222,15 @@
                 remote(block, block, dz_send, dz_recv.at[j, src], sp=src).wait_recv()
             down_y(j, src, g, me).start()
 
+    inputs = [
+        pltpu.make_async_copy(src, dst, in_sem.at[i])
+        for i, (src, dst) in enumerate((
+            (k_hbm, k_ref), (v_hbm, v_ref), (q_hbm, q_ref), (gate_t_hbm, gate_t_ref),
+            (gain_hbm, gain_ref), (resid_hbm, resid_ref),
+        ))
+    ]
+    for copy in inputs:
+        copy.start()
     barrier = pltpu.get_barrier_semaphore()
 
     def greet(i):
@@ -227,6 +243,8 @@
         pl.semaphore_signal(barrier, inc=1, device_id={"tp": (t + j) % nt}, device_id_type=MESH)
     with sc("bar"):
         pl.semaphore_wait(barrier, ns + nt - 1)
+        for copy in inputs[:4]:
+            copy.wait()
 
     def kv_out(i, kk, vv):
         return (
@@ -353,6 +371,8 @@
 
     with sc("mix"):
         w_out_copy.wait()
+        for copy in inputs[4:]:
+            copy.wait()
         resid[...] = resid_ref[...].astype(F32) + jnp.dot(
             att[pl.ds(pl.multiple_of(t * rows, rows), rows), :],
             w_out[pl.ds(pl.multiple_of(t * att_w, att_w), att_w), :], preferred_element_type=F32,
@@ -532,6 +552,9 @@
         elif u == nu - 1 and me == 0:
             for j in range(1, nj):
                 send_down(0, j, 2, 3)
+        if (me, u) in ((0, nu - 1), (1, nu - 1), (2, nu - 1), (3, 1)):
+            for j in range(1, nj):
+                pass_down(me, j, me ^ 1)
 
     def own_units(u):
         def body(me):
@@ -599,7 +622,7 @@
             hide(u, ns - 1, ns)
 
     def pass_down_all(j):
-        on_each_s(lambda me: pass_down(me, j, me ^ 1, me ^ 2, me ^ 3))
+        on_each_s(lambda me: pass_down(me, j, me ^ 2, me ^ 3))
 
     steps = [(0, m) for m in (3, 1, 2, 0)]
     steps += [(j, m) for j in range(1, nj - 2) for m in (3, 1, 2)]
@@ -615,10 +638,15 @@
     def sum_x(d):
         return remote(csend.at[d], xrecv.at[d], rx_send, rx_recv.at[d], tp=tx)
 
-    def sum_z(d):
+    def sum_near(d):
         i = slot[d]
-        to = xor(s, 2 if steps[d][1] == 2 else 1)
-        return remote(zsend.at[i], zrecv.at[i], rz_send, rz_recv.at[i], sp=to)
+        return remote(zsend.at[i], zrecv.at[i], rz_send, rz_recv.at[i], sp=xor(s, 1))
+
+    def sum_on(d):
+        j, m = steps[d]
+        return remote(zsend.at[slot[d]], frecv.at[j], rz_send, rf_recv.at[j], sp=xor(s, m))
+
+    middle = (s > 0) & (s < ns - 1)
 
     def stage_x(d):
         sum_c(d).wait_recv()
@@ -627,17 +655,26 @@
         keep[d] = part[d, x, c].astype(F32) + crecv[d, x].astype(F32)
 
     def stage_z(d):
-        j, m = steps[d]
+        m = steps[d][1]
         if m == 0:
             return
         sum_x(d).wait_recv()
-        total = keep[d] + xrecv[d].astype(F32)
-        if m == 2:
-            from_near = at[j, 3]
-            sum_z(from_near).wait_recv()
-            total = total + zrecv[slot[from_near]].astype(F32)
-        zsend[slot[d]] = total.astype(BF16)
-        sum_z(d).start()
+        keep[d] = keep[d] + xrecv[d].astype(F32)
+
+        @pl.when((m == 1) | ~middle)
+        def _():
+            zsend[slot[d]] = keep[d].astype(BF16)
+            sum_near(d).start()
+
+    def stage_on(d):
+        j, m = steps[d]
+
+        @pl.when(middle)
+        def _():
+            other = at[j, 5 - m]
+            sum_near(other).wait_recv()
+            zsend[slot[d]] = (keep[d] + zrecv[slot[other]].astype(F32)).astype(BF16)
+            sum_on(d).start()
 
     def feed(d):
         j, m = steps[d]
@@ -653,17 +690,20 @@
         sum_c(d).start()
 
     def finish(j):
-        d, near, far = at[j, 0], at[j, 1], at[j, 2]
+        d, near = at[j, 0], at[j, 1]
         sum_x(d).wait_recv()
-        sum_z(near).wait_recv()
-        sum_z(far).wait_recv()
+        sum_near(near).wait_recv()
+        remote(frecv.at[j], frecv.at[j], rz_send, rf_recv.at[j], sp=xor(s, 1)).wait_recv()
         total = (
-            keep[d] + xrecv[d].astype(F32) + zrecv[slot[near]].astype(F32)
-            + zrecv[slot[far]].astype(F32)
+            keep[d] + xrecv[d].astype(F32) + zrecv[slot[near]].astype(F32) + frecv[j].astype(F32)
         )
         for p in range(ns):
             cols = slice(p * depth + j * dj, p * depth + (j + 1) * dj)
             out_ref[:, cols] = (resid[:, cols] + total[:, p * dj : (p + 1) * dj]).astype(BF16)
+
+    def on_time(i):
+        j, m = steps[i]
+        return {2: at[j, 2] + 4, 3: at[j, 2] + 7}.get(m, -1)
 
     ready = set()
     for d in range(nd):
@@ -677,16 +717,25 @@
             feed(d)
             if d >= 1:
                 stage_x(d - 1)
-        if 2 <= d <= nj:
-            with sc(f"pd{d - 1}"):
-                pass_down_all(d - 1)
-        if d >= 3:
-            with sc(f"z{d}"):
-                stage_z(d - 3)
+        ahead = d - 1 if 2 <= d <= nj else nj
+        if ahead < nj:
+            with sc(f"pd{ahead}"):
+                pass_down_all(ahead)
+        for i in range(nd):
+            if d == i + 4:
+                with sc(f"z{i}"):
+                    stage_z(i)
+        for i in range(nd):
+            if d == on_time(i):
+                with sc(f"o{i}"):
+                    stage_on(i)
     with sc("st"):
         stage_x(nd - 1)
-        for d in range(nd - 3, nd):
-            stage_z(d)
+        for d in range(nd, nd + 4):
+            stage_z(d - 4)
+            for i in range(nd):
+                if d == on_time(i):
+                    stage_on(i)
     for j in range(nj):
         with sc(f"fin{j}"):
             finish(j)
@@ -737,9 +786,15 @@
     return pl.pallas_call(
         functools.partial(layer_kernel, (ns, nt, chunk, nj)),
         out_shape=jax.ShapeDtypeStruct((rows, width), BF16),
-        in_specs=[vm] * 6 + [hbm] * 4,
+        in_specs=[hbm] * 10,
         out_specs=vm,
         scratch_shapes=[
+            pltpu.VMEM((rows, width), BF16),
+            pltpu.VMEM((tok, att_w), BF16),
+            pltpu.VMEM((tok, att_w), BF16),
+            pltpu.VMEM((tok, att_w), BF16),
+            pltpu.VMEM(cum_gate.shape[::-1], F32),
+            pltpu.VMEM((1, width), F32),
             pltpu.VMEM((ns - 1, tok, att_w), BF16),
             pltpu.VMEM((ns - 1, tok, att_w), BF16),
             pltpu.VMEM((nheads, tok, 1), F32),
@@ -760,9 +815,11 @@
             pltpu.VMEM((nd, rows, wide), BF16),
             pltpu.VMEM((3 * nj, rows, wide), BF16),
             pltpu.VMEM((3 * nj, rows, wide), BF16),
+            pltpu.VMEM((nj, rows, wide), BF16),
+            dma((6,)),
             dma((1 + 2 * nu + nj,)),
             dma((2,)), dma((2, ns - 1)),
-            dma, dma((nu, ns)),
+            dma, dma((nu + 1, ns)),
             dma, dma((nu,)),
             dma, dma((nj, ns)),
             dma, dma((nj,)),
@@ -773,6 +830,7 @@
             dma, dma((nd,)),
             dma, dma((nd,)),
             dma, dma((3 * nj,)),
+            dma((nj,)),
         ],
         compiler_params=pltpu.CompilerParams(
             collective_id=0, has_side_effects=True, vmem_limit_bytes=60 * 2**20

time: 102 us -> 99.8 us (0.978)
  Pallas kernels: 100 us -> 98 us
    pallas_call x1, Pallas kernels: 100 us -> 98 us  [fused(): pl.pallas_call(functools.partial(layer_kernel, (ns, nt, chunk, nj)), out_...]
where the time goes in v4:
time: 99.8 us; the launch traced here: 99.7 us
  Pallas kernels  98 us (98%)
  local copies, waits for them, and re-layouts  1.67 us (2%)
    pallas_call x1, Pallas kernels, fused(): pl.pallas_call(functools.partial(layer_kernel, (ns, nt, chunk, nj)), out_...  98 us

profile of v4, /device:TPU:0, one launch (start us, length us, event | category | flops | bytes accessed | tf_op | source)
XLA Modules:
  0.0 99.7 jit_solution(11489888005888069445)
XLA Ops:
  0.0 98.0 %layer.1 = bf16[64,2048]{1,0:T(8,128)(2,1)} custom-call(bf16[64,2048]{1,0:T(8,128)(2,1)} %resid_hbm.1, bf16[256,256]{1,0:T(8,128)(2,1)} %q_hbm.1, bf16[256,256]{1,0:T(8,128)(2,1)} %k_hbm.1, bf16[256,256]{1,0:T(8,128)(2,1)} %v_hbm.1, f32[4,1024]{1,0:T(4,128)} %bitcast.2, f32[1,2048]{1,0:T(1,128)} %bitcast.3, bf16[1024,2048]{1,0:T(8,128)(2,1)} %w_out_ref.1, ...), custom_call_target="tpu_custom_call" | custom-call | tf_op jit(solution)/shard_map/layer/pallas_call | solution.py:786
  98.0 1.7 %copy.12 = bf16[64,2048]{1,0:T(8,128)(2,1)} copy(bf16[64,2048]{1,0:T(8,128)(2,1)} %layer.1) | data formatting | bytes 524288

commit v5 on v4

--- a/solution.py
+++ b/solution.py
@@ -625,9 +625,7 @@
         on_each_s(lambda me: pass_down(me, j, me ^ 2, me ^ 3))
 
     steps = [(0, m) for m in (3, 1, 2, 0)]
-    steps += [(j, m) for j in range(1, nj - 2) for m in (3, 1, 2)]
-    steps += [(j, m) for m in (3, 2, 1) for j in (nj - 2, nj - 1)]
-    steps += [(j, 0) for j in range(1, nj)]
+    steps += [(j, m) for m in (3, 2, 1, 0) for j in range(1, nj)]
     nd = len(steps)
     at = {step: d for d, step in enumerate(steps)}
     slot = {d: i for i, d in enumerate(d for d in range(nd) if steps[d][1])}

time: 99.8 us -> 99.5 us (level)
  no operation moved by 1% of the time
where the time goes in v5:
time: 99.5 us; the launch traced here: 99.3 us
  Pallas kernels  97.6 us (98%)
  local copies, waits for them, and re-layouts  1.67 us (2%)
    pallas_call x1, Pallas kernels, fused(): pl.pallas_call(functools.partial(layer_kernel, (ns, nt, chunk, nj)), out_...  97.6 us

profile of v5, /device:TPU:0, one launch (start us, length us, event | category | flops | bytes accessed | tf_op | source)
XLA Modules:
  0.0 99.3 jit_solution(2851045322484926597)
XLA Ops:
  0.0 97.6 %layer.1 = bf16[64,2048]{1,0:T(8,128)(2,1)} custom-call(bf16[64,2048]{1,0:T(8,128)(2,1)} %resid_hbm.1, bf16[256,256]{1,0:T(8,128)(2,1)} %q_hbm.1, bf16[256,256]{1,0:T(8,128)(2,1)} %k_hbm.1, bf16[256,256]{1,0:T(8,128)(2,1)} %v_hbm.1, f32[4,1024]{1,0:T(4,128)} %bitcast.2, f32[1,2048]{1,0:T(1,128)} %bitcast.3, bf16[1024,2048]{1,0:T(8,128)(2,1)} %w_out_ref.1, ...), custom_call_target="tpu_custom_call" | custom-call | tf_op jit(solution)/shard_map/layer/pallas_call | solution.py:784
  97.6 1.7 %copy.12 = bf16[64,2048]{1,0:T(8,128)(2,1)} copy(bf16[64,2048]{1,0:T(8,128)(2,1)} %layer.1) | data formatting | bytes 524288

commit v6 on v5

--- a/solution.py
+++ b/solution.py
@@ -404,18 +404,18 @@
         block = half_of(src, who, h)
         return remote(block, block, ax_send, ax_recv.at[src, h], tp=tx)
 
-    def row_c(kind, src, who, h):
+    def row_c(src, who, h):
         block = half_of(src, who, h)
-        return remote(block, block, ac_send, ac_recv.at[kind, src, h], tp=tc)
+        return remote(block, block, ac_send, ac_recv.at[src], tp=tc)
 
     def spread(src, h):
         row_x(src, t, h).start()
-        row_c(0, src, t, h).start()
+        row_c(src, t, h).start()
 
     def relay(src):
         for h in range(2):
             row_x(src, tx, h).wait_recv()
-            row_c(1, src, tx, h).start()
+            row_c(src, tx, h).start()
 
     def take(me, src):
         for h in range(2):
@@ -601,9 +601,8 @@
 
     def rows_in(i):
         k = jnp.where(i == ns - 1, final, i + jnp.where(i >= final, 1, 0))
-        for h in range(2):
-            row_c(0, k, tc, h).wait_recv()
-            row_c(1, k, (tc + 2) % 4, h).wait_recv()
+        both = nall.at[k, pl.ds(0, 2)]
+        remote(both, both, ac_send, ac_recv.at[k], tp=tc).wait_recv()
 
     with sc("rows"):
         each(0, ns - 1, rows_in)
@@ -766,7 +765,7 @@
 
         remote(nall.at[0], nall.at[0], ax_send, ax_recv.at[0, 0], tp=tx).wait_send()
         sent = nall.at[pl.ds(0, 2)]
-        remote(sent, sent, ac_send, ac_recv.at[0, 0, 0], tp=tx).wait_send()
+        remote(sent, sent, ac_send, ac_recv.at[0], tp=tx).wait_send()
         remote(crecv, crecv, rc_send, rc_recv.at[0], tp=tc).wait_send()
         remote(xrecv, xrecv, rx_send, rx_recv.at[0], tp=tx).wait_send()
         remote(zrecv, zrecv, rz_send, rz_recv.at[0], tp=tx).wait_send()
@@ -824,7 +823,7 @@
             dma, dma((nt - 1,)),
             dma, dma((ns, 2)),
             dma, dma((ns, 2)),
-            dma, dma((2, ns, 2)),
+            dma, dma((ns,)),
             dma, dma((nd,)),
             dma, dma((nd,)),
             dma, dma((3 * nj,)),

time: 99.5 us -> 99.4 us (level)
  no operation moved by 1% of the time
where the time goes in v6:
time: 99.4 us; the launch traced here: 99.2 us
  Pallas kernels  97.5 us (98%)
  local copies, waits for them, and re-layouts  1.67 us (2%)
    pallas_call x1, Pallas kernels, fused(): pl.pallas_call(functools.partial(layer_kernel, (ns, nt, chunk, nj)), out_...  97.5 us

profile of v6, /device:TPU:0, one launch (start us, length us, event | category | flops | bytes accessed | tf_op | source)
XLA Modules:
  0.0 99.2 jit_solution(11994361891760950510)
XLA Ops:
  0.0 97.5 %layer.1 = bf16[64,2048]{1,0:T(8,128)(2,1)} custom-call(bf16[64,2048]{1,0:T(8,128)(2,1)} %resid_hbm.1, bf16[256,256]{1,0:T(8,128)(2,1)} %q_hbm.1, bf16[256,256]{1,0:T(8,128)(2,1)} %k_hbm.1, bf16[256,256]{1,0:T(8,128)(2,1)} %v_hbm.1, f32[4,1024]{1,0:T(4,128)} %bitcast.2, f32[1,2048]{1,0:T(1,128)} %bitcast.3, bf16[1024,2048]{1,0:T(8,128)(2,1)} %w_out_ref.1, ...), custom_call_target="tpu_custom_call" | custom-call | tf_op jit(solution)/shard_map/layer/pallas_call | solution.py:783
  97.5 1.7 %copy.12 = bf16[64,2048]{1,0:T(8,128)(2,1)} copy(bf16[64,2048]{1,0:T(8,128)(2,1)} %layer.1) | data formatting | bytes 524288
